TPU v7x, 32 devices: a whole 2x2x4 slice. The times are simulated.
32 devices in a mesh: ep: 8 (over z, x), tp: 4 (over y, core).
Axes of the slice: x: 2, y: 2, z: 4, core: 2. Of those that a mesh axis runs over, the one named last changes fastest.
Arguments:
- q_in: bfloat16 [4096, 1024], P('ep', 'tp'), may hold values from -6 to 6
- k_in: bfloat16 [4096, 256], P('ep'), may hold values from -6 to 6
- v_in: bfloat16 [4096, 256], P('ep'), may hold values from -6 to 6
- q_gain: float32 [64], replicated, may hold values from 0.1 to 1.9
- k_gain: float32 [64], replicated, may hold values from 0.1 to 1.9
- w_out: bfloat16 [1024, 2048], P('tp'), may hold values from -0.1875 to 0.1875
- post_gain: float32 [2048], replicated, may hold values from 0.1 to 1.9
- moe_in: bfloat16 [1024, 2048], P('ep'), may hold values from -6 to 6
- routes: int32 [1024, 2], P('ep'), may hold values from 0 to 7, all different within a row; in each aligned block of 128 rows (0 to 127, 128 to 255, ...) at most 48 rows name the same one
- route_logits: float32 [1024, 2], P('ep'), may hold values from -6 to 6
- pre_gain: float32 [2048], replicated, may hold values from 0.1 to 1.9
- w_gate: bfloat16 [8, 2048, 4096], P('ep', None, 'tp'), may hold values from -0.125 to 0.125
- w_up: bfloat16 [8, 2048, 4096], P('ep', None, 'tp'), may hold values from -0.125 to 0.125
- w_down: bfloat16 [8, 4096, 2048], P('ep', 'tp'), may hold values from -0.125 to 0.125
Outputs:
- attn_out: bfloat16 [4096, 2048], P(('ep', 'tp'))
- moe_out: bfloat16 [1024, 2048], P('ep', 'tp')
Inputs may be any that keep to these rules, and one draw needn't show every extreme that they name: `routes`: each row names 2 different experts. Among the rows of one index of ep no expert is named by more than 48 rows, a bound that some block reaches of them.
All inputs are finite; a program needn't handle non-finite values.
Results may differ from a plain program's by a relative error of at most 0.018.
Values may be sent and summed in bfloat16 or wider, within the bound.
A program may use at most 64 MiB of HBM per device.

v0:
```python
import functools

import jax
import jax.numpy as jnp
from jax import lax
from jax.experimental import pallas as pl
from jax.experimental.pallas import tpu as pltpu
from jax.sharding import PartitionSpec as P

GRID_W = 128
EPSILON = 1e-06
ROPE_BASE = 10000.0
MESH = pl.DeviceIdType.MESH


def head_norm(values, gain):
    return values * lax.rsqrt(jnp.mean(values * values, axis=-1, keepdims=True) + EPSILON) * gain


def rotate_half(values, angles):
    quarter = angles.shape[-1]
    first_part = values[..., :quarter]
    second_part = values[..., quarter:]
    cosine = jnp.cos(angles)[:, None, :]
    sine_part = jnp.sin(angles)[:, None, :]
    return jnp.concatenate(
        [
            first_part * cosine - second_part * sine_part,
            second_part * cosine + first_part * sine_part,
        ],
        axis=-1,
    )


def grid_rotary(values, offset):
    row_count = values.shape[0]
    head_width = values.shape[-1]
    quarter = head_width // 4
    half_width = head_width // 2
    position = offset + jnp.arange(row_count, dtype=jnp.int32)
    grid_row = (position // GRID_W).astype(jnp.float32)
    grid_col = (position % GRID_W).astype(jnp.float32)
    inverse = ROPE_BASE ** (-jnp.arange(quarter, dtype=jnp.float32) / quarter)
    return jnp.concatenate(
        [
            rotate_half(values[..., :half_width], grid_row[:, None] * inverse[None, :]),
            rotate_half(values[..., half_width:], grid_col[:, None] * inverse[None, :]),
        ],
        axis=-1,
    )


def kernel(
    dims,
    q_ref, pair_ref, x_ref, route_ref, logit_ref, pre_ref, ids_ref, wout_ref, gain_ref, wg_hbm, wu_hbm, wd_hbm,
    attn_ref, moe_ref,
    outgo_ref, mixw_ref, wg, wu, wd, kvbuf, vx, kt, acc, arrived, hidden,
    pa, pa_in, pa_red, pa_in2, pm, pm_in, pm_red, pm_in2, summed, ret,
    w_sem, loc_sem, kv_s, kv_r, disp_s, disp_r, rel_s, rel_r, fwd_s,
    a1_s, a1_r, a2_s, a2_r, m1_s, m1_r, m2_s, m2_r, ret_s, ret_r,
):
    n_ep, n_tp, heads, cap = dims
    ny = n_tp // 2
    ep = lax.axis_index("ep")
    tp = lax.axis_index("tp")
    core = lax.rem(tp, 2)
    row = tp // 2
    partner = row * 2 + 1 - core
    rows_kv = pair_ref.shape[0]
    dq = outgo_ref.shape[1]
    slots = outgo_ref.shape[0]
    piece = attn_ref.shape[0]

    def remote(src, dst, ss, rs, e, t):
        return pltpu.make_async_remote_copy(
            src_ref=src, dst_ref=dst, send_sem=ss, recv_sem=rs,
            device_id=(e, t), device_id_type=MESH,
        )

    def ep_at(d):
        return lax.rem(ep + d, n_ep)

    def ep_from(d):
        return lax.rem(ep - d + n_ep, n_ep)

    def same_core(d):
        return lax.rem(row + d, ny) * 2 + core

    def row_from(d):
        return lax.rem(row - d + ny, ny)

    def slot_rows(e):
        return pl.ds(pl.multiple_of(e * cap, cap), cap)

    loads = [
        pltpu.make_async_copy(src, dst, w_sem.at[i])
        for i, (src, dst) in enumerate(((wg_hbm, wg), (wu_hbm, wu), (wd_hbm, wd)))
    ]
    barrier = pltpu.get_barrier_semaphore()
    for d in range(1, n_ep):
        pl.semaphore_signal(barrier, inc=1, device_id=(ep_at(d), tp), device_id_type=MESH)
    for d in range(1, ny):
        pl.semaphore_signal(barrier, inc=1, device_id=(ep, same_core(d)), device_id_type=MESH)
    pl.semaphore_signal(barrier, inc=1, device_id=(ep, partner), device_id_type=MESH)

    x = x_ref[...].astype(jnp.float32)
    scale = lax.rsqrt(jnp.mean(x * x, axis=-1, keepdims=True) + EPSILON)
    mine = pl.ds(pl.multiple_of(tp * dq, dq), dq)
    normed = (x_ref[:, mine].astype(jnp.float32) * scale * pre_ref[:, mine]).astype(jnp.bfloat16)
    logits = logit_ref[...]
    top = logits.shape[1]
    tokens = logits.shape[0]
    power = jnp.exp(logits - jnp.max(logits, axis=1, keepdims=True))
    chance = power / jnp.sum(power, axis=1, keepdims=True)
    named = jnp.zeros((tokens, slots), jnp.float32)
    share = jnp.zeros((tokens, slots), jnp.float32)
    for j in range(top):
        hit = route_ref[:, j : j + 1] == ids_ref[0:1, :]
        named = jnp.where(hit, 1.0, named)
        share = jnp.where(hit, chance[:, j : j + 1], share)
    below = lax.broadcasted_iota(jnp.int32, (tokens, tokens), 1) < lax.broadcasted_iota(
        jnp.int32, (tokens, tokens), 0
    )
    rank = jnp.dot(
        jnp.where(below, 1.0, 0.0).astype(jnp.bfloat16), named.astype(jnp.bfloat16),
        preferred_element_type=jnp.float32,
    )
    placed = jnp.where(rank == ids_ref[1:2, :].astype(jnp.float32), named, 0.0)
    mixw_ref[...] = placed * share
    outgo_ref[...] = lax.dot_general(
        placed.astype(jnp.bfloat16), normed, (((0,), (0,)), ((), ())),
        preferred_element_type=jnp.float32,
    ).astype(jnp.bfloat16)
    own = pltpu.make_async_copy(
        outgo_ref.at[slot_rows(ep)], arrived.at[tp, slot_rows(ep)], loc_sem.at[0]
    )
    own.start()
    pl.semaphore_wait(barrier, n_ep - 1 + ny - 1 + 1)

    disp = [
        remote(outgo_ref.at[slot_rows(ep_at(d))], arrived.at[tp, slot_rows(ep)],
               disp_s.at[d], disp_r.at[d], ep_at(d), tp)
        for d in range(1, n_ep)
    ]
    nz = n_ep // 2
    side = lax.rem(ep, 2)
    col = ep // 2
    mate = col * 2 + 1 - side

    def col_from(d, which):
        return lax.rem(col - d + nz, nz) * 2 + which

    def kv_direct(d):
        return remote(pair_ref, kvbuf.at[ep], kv_s.at[d], kv_r.at[d],
                      lax.rem(col + d, nz) * 2 + side, tp)

    def kv_pass(d):
        held = kvbuf.at[col_from(d, side)]
        return remote(held, held, kv_s.at[nz + d], kv_r.at[nz + d], mate, tp)

    kv_mate = remote(pair_ref, kvbuf.at[ep], kv_s.at[nz], kv_r.at[nz], mate, tp)
    kv_mate.start()
    for copy in disp:
        copy.start()
    for d in range(1, nz):
        kv_direct(d).start()
    for copy in loads:
        copy.start()

    q_rows = q_ref.shape[0]
    tile = min(512, q_rows // 2)

    def attend(keys_of, first):
        keys = keys_of[...]
        lanes = lax.broadcasted_iota(jnp.int32, keys.shape, 1)
        kt[...] = keys.T
        vx[...] = jnp.where(lanes < keys.shape[1] // 2, jnp.ones_like(keys), keys)

        def one(i, carry):
            for sub in range(2):
                at = pl.ds(pl.multiple_of(i * 2 * tile + sub * tile, tile), tile)
                scores = jnp.dot(q_ref[at, :], kt[...], preferred_element_type=jnp.float32)
                weights = jnp.exp(scores).astype(jnp.bfloat16)
                term = jnp.dot(weights, vx[...], preferred_element_type=jnp.float32)
                if first:
                    acc[at, :] = term
                else:
                    acc[at, :] += term
            return carry

        lax.fori_loop(0, q_rows // (2 * tile), one, 0)

    attend(pair_ref, True)

    kv_mate.wait_recv()
    attend(kvbuf.at[mate], False)

    def later(d, carry):
        kv_direct(d).wait_recv()
        kv_pass(d).start()
        attend(kvbuf.at[col_from(d, side)], False)
        kv_pass(d).wait_recv()
        attend(kvbuf.at[col_from(d, 1 - side)], False)
        return carry

    early = 1 + (nz - 1) // 3
    late = max(early, nz - 1)
    lax.fori_loop(1, early, later, 0)

    own.wait()
    for copy in disp:
        copy.wait_recv()
    relay = [
        remote(arrived.at[tp], arrived.at[tp], rel_s.at[d], rel_r.at[d], ep, same_core(d))
        for d in range(1, ny)
    ]
    cross = [
        remote(arrived.at[row_from(d) * 2 + core], arrived.at[row_from(d) * 2 + core],
               fwd_s.at[d], rel_r.at[ny + d], ep, partner)
        for d in range(ny)
    ]
    for copy in relay:
        copy.start()
    cross[0].start()
    lax.fori_loop(early, late, later, 0)
    for d in range(1, ny):
        relay[d - 1].wait_recv()
        cross[d].start()
    lax.fori_loop(late, nz, later, 0)

    outs = []
    tokens = q_rows // heads
    half = acc.shape[1] // 2
    for j in range(n_tp):
        pieces = []
        for h in range(heads):
            a = acc[h * tokens + j * piece : h * tokens + (j + 1) * piece, :]
            pieces.append((a[:, half:] / a[:, :half]).astype(jnp.bfloat16))
        mine = pieces[0] if heads == 1 else jnp.concatenate(pieces, axis=1)
        pa[j % 2, j // 2] = jnp.dot(
            mine, wout_ref[...], preferred_element_type=jnp.float32
        ).astype(jnp.bfloat16)
    a1 = remote(pa.at[1 - core], pa_in, a1_s.at[0], a1_r.at[0], ep, partner)
    a1.start()

    for copy in cross:
        copy.wait_recv()
    loads[0].wait()
    loads[1].wait()
    a1.wait_recv()
    for y in range(ny):
        pa_red[y] = (
            pa[core, y].astype(jnp.float32) + pa_in[y].astype(jnp.float32)
        ).astype(jnp.bfloat16)
    a2 = [
        remote(pa_red.at[lax.rem(row + d, ny)], pa_in2.at[row],
               a2_s.at[d], a2_r.at[d], ep, same_core(d))
        for d in range(1, ny)
    ]
    for copy in a2:
        copy.start()

    ff = hidden.shape[1]
    step = min(256, ff)

    def gated(i, carry):
        at = pl.ds(pl.multiple_of(i * step, step), step)
        gate = jnp.zeros((slots, step), jnp.float32)
        up = jnp.zeros((slots, step), jnp.float32)
        for q in range(n_tp):
            x = arrived[q]
            gate = gate + jnp.dot(x, wg[q * dq : (q + 1) * dq, at], preferred_element_type=jnp.float32)
            up = up + jnp.dot(x, wu[q * dq : (q + 1) * dq, at], preferred_element_type=jnp.float32)
        hidden[:, at] = (gate / (1.0 + jnp.exp(-gate)) * up).astype(jnp.bfloat16)
        return carry

    lax.fori_loop(0, ff // step, gated, 0)
    loads[2].wait()

    def down_for(which):
        def down(y, carry):
            cols = pl.ds(pl.multiple_of((y * 2 + which) * dq, dq), dq)
            pm[which, y] = jnp.dot(
                hidden[...], wd[:, cols], preferred_element_type=jnp.float32
            ).astype(jnp.bfloat16)
            return carry

        lax.fori_loop(0, ny, down, 0)

    m1 = remote(pm.at[1 - core], pm_in, m1_s.at[0], m1_r.at[0], ep, partner)
    down_for(1 - core)
    m1.start()
    down_for(core)
    m1.wait_recv()
    for y in range(ny):
        pm_red[y] = (
            pm[core, y].astype(jnp.float32) + pm_in[y].astype(jnp.float32)
        ).astype(jnp.bfloat16)
    m2 = [
        remote(pm_red.at[lax.rem(row + d, ny)], pm_in2.at[row],
               m2_s.at[d], m2_r.at[d], ep, same_core(d))
        for d in range(1, ny)
    ]
    for copy in m2:
        copy.start()

    for copy in a2:
        copy.wait_recv()
    mixed = pa_red[row].astype(jnp.float32)
    for d in range(1, ny):
        mixed = mixed + pa_in2[row_from(d)].astype(jnp.float32)
    square = jnp.mean(mixed * mixed, axis=-1, keepdims=True)
    attn_ref[...] = (mixed * lax.rsqrt(square + EPSILON) * gain_ref[...]).astype(jnp.bfloat16)

    for copy in m2:
        copy.wait_recv()
    total = pm_red[row].astype(jnp.float32)
    for d in range(1, ny):
        total = total + pm_in2[row_from(d)].astype(jnp.float32)
    summed[...] = total.astype(jnp.bfloat16)
    back = [
        remote(summed.at[slot_rows(ep_at(d))], ret.at[slot_rows(ep)],
               ret_s.at[d], ret_r.at[d], ep_at(d), tp)
        for d in range(1, n_ep)
    ]
    for copy in back:
        copy.start()
    mine = pltpu.make_async_copy(
        summed.at[slot_rows(ep)], ret.at[slot_rows(ep)], loc_sem.at[1]
    )
    mine.start()
    mine.wait()
    for copy in back:
        copy.wait_recv()
    mixw = mixw_ref[...]
    high = mixw.astype(jnp.bfloat16)
    low = (mixw - high.astype(jnp.float32)).astype(jnp.bfloat16)
    moe_ref[...] = (
        jnp.dot(high, ret[...], preferred_element_type=jnp.float32)
        + jnp.dot(low, ret[...], preferred_element_type=jnp.float32)
    ).astype(jnp.bfloat16)

    for copy in [kv_mate] + disp + relay + cross + [a1] + a2 + [m1] + m2 + back:
        copy.wait_send()

    def kv_done(d, carry):
        kv_direct(d).wait_send()
        kv_pass(d).wait_send()
        return carry

    lax.fori_loop(1, nz, kv_done, 0)


def per_device(
    n_ep, n_tp,
    q_in, k_in, v_in, q_gain, k_gain, w_out, post_gain,
    moe_in, routes, route_logits, pre_gain, w_gate, w_up, w_down,
):
    bf16 = jnp.bfloat16
    head = q_gain.shape[0]
    rows = q_in.shape[0]
    heads = q_in.shape[1] // head
    kv_count = k_in.shape[1] // head
    repeat = heads * n_tp // kv_count
    ny = n_tp // 2
    offset = lax.axis_index("ep") * rows
    queries = head_norm(q_in.astype(jnp.float32).reshape(rows, heads, head), q_gain)
    queries = grid_rotary(queries, offset).astype(bf16) * jnp.asarray(head ** (-0.5), bf16)
    queries = jnp.transpose(queries, (1, 0, 2)).reshape(heads * rows, head)
    queries = jnp.concatenate([queries, jnp.zeros_like(queries)], axis=1)
    kv_index = lax.axis_index("tp") * heads // repeat
    keys = lax.dynamic_slice_in_dim(k_in, kv_index * head, head, 1)
    values = lax.dynamic_slice_in_dim(v_in, kv_index * head, head, 1)
    keys = head_norm(keys.astype(jnp.float32)[:, None, :], k_gain)
    keys = grid_rotary(keys, offset)[:, 0, :].astype(bf16)
    paired = jnp.concatenate([keys, values], axis=1)

    tokens, top = routes.shape
    width = moe_in.shape[1]
    dq = width // n_tp
    need = max(2, 3 * top * tokens // (2 * n_ep))
    cap = -(-need // 16) * 16
    slots = n_ep * cap
    slot = jnp.arange(slots, dtype=jnp.int32)
    ids = jnp.stack([slot // cap, slot % cap])

    piece = rows // n_tp
    ff = w_gate.shape[2]
    dma = pltpu.SemaphoreType.DMA
    vmem = pl.BlockSpec(memory_space=pltpu.VMEM)
    hbm = pl.BlockSpec(memory_space=pl.ANY)
    return pl.pallas_call(
        functools.partial(kernel, (n_ep, n_tp, heads, cap)),
        out_shape=(
            jax.ShapeDtypeStruct((piece, width), bf16),
            jax.ShapeDtypeStruct((tokens, dq), bf16),
        ),
        in_specs=[vmem] * 9 + [hbm] * 3,
        out_specs=(vmem, vmem),
        scratch_shapes=[
            pltpu.VMEM((slots, dq), bf16),
            pltpu.VMEM((tokens, slots), jnp.float32),
            pltpu.VMEM((width, ff), bf16),
            pltpu.VMEM((width, ff), bf16),
            pltpu.VMEM((ff, width), bf16),
            pltpu.VMEM((n_ep, rows, 2 * head), bf16),
            pltpu.VMEM((rows, 2 * head), bf16),
            pltpu.VMEM((2 * head, rows), bf16),
            pltpu.VMEM((heads * rows, 2 * head), jnp.float32),
            pltpu.VMEM((n_tp, slots, dq), bf16),
            pltpu.VMEM((slots, ff), bf16),
            pltpu.VMEM((2, ny, piece, width), bf16),
            pltpu.VMEM((ny, piece, width), bf16),
            pltpu.VMEM((ny, piece, width), bf16),
            pltpu.VMEM((ny, piece, width), bf16),
            pltpu.VMEM((2, ny, slots, dq), bf16),
            pltpu.VMEM((ny, slots, dq), bf16),
            pltpu.VMEM((ny, slots, dq), bf16),
            pltpu.VMEM((ny, slots, dq), bf16),
            pltpu.VMEM((slots, dq), bf16),
            pltpu.VMEM((slots, dq), bf16),
            dma((3,)), dma((2,)),
            dma((n_ep,)), dma((n_ep,)), dma((n_ep,)), dma((n_ep,)),
            dma((ny,)), dma((2 * ny,)), dma((ny,)),
            dma((1,)), dma((1,)), dma((ny,)), dma((ny,)),
            dma((1,)), dma((1,)), dma((ny,)), dma((ny,)),
            dma((n_ep,)), dma((n_ep,)),
        ],
        compiler_params=pltpu.CompilerParams(
            collective_id=0, has_side_effects=True, vmem_limit_bytes=60 * 1024 * 1024
        ),
    )(queries, paired, moe_in, routes, route_logits, pre_gain[None, :], ids, w_out, post_gain[None, :], w_gate[0], w_up[0], w_down[0])


def solution(mesh):
    return jax.shard_map(
        functools.partial(per_device, mesh.shape["ep"], mesh.shape["tp"]),
        mesh=mesh,
        in_specs=(
            P("ep", "tp"),
            P("ep", None),
            P("ep", None),
            P(),
            P(),
            P("tp", None),
            P(),
            P("ep", None),
            P("ep", None),
            P("ep", None),
            P(),
            P("ep", None, "tp"),
            P("ep", None, "tp"),
            P("ep", "tp", None),
        ),
        out_specs=(P(("ep", "tp"), None), P("ep", "tp")),
        check_vma=False,
    )
```

profile of v0, /device:TPU:0, one launch (start us, length us, event | category | flops | bytes accessed | tf_op | source)
XLA Modules:
  0.0 88.7 jit_solution(11897758026393704382)
XLA Ops:
  0.6 0.0 copy-start
  0.6 0.0 copy-start.1
  0.7 1.2 %fusion.10 = f32[512]{0:T(512)S(1)} fusion(bf16[512,256]{1,0:T(8,128)(2,1)} %param.15, s32[]{:T(128)S(6)} %select_n.59), kind=kLoop, calls=%fused_computation.18 | loop fusion | flops 97792 | bytes 67588 | tf_op jit(solution)/shard_map/reduce_sum | solution.py:17
  1.9 0.6 pad_add_fusion.ids_ref
  2.5 1.4 %copy.27.route_ref = s32[128,2]{1,0:T(8,128)} copy(s32[128,2]{0,1:T(2,128)} %param.22) | data formatting | bytes 2048 | tf_op args[8]
  3.9 1.4 %copy.28.logit_ref = f32[128,2]{1,0:T(8,128)} copy(f32[128,2]{0,1:T(2,128)} %param.23) | data formatting | bytes 2048 | tf_op args[9]
  5.3 0.0 copy-done
  5.3 0.1 constant_dynamic-slice_fusion
  5.4 0.3 multiply_cosine_fusion.3
  5.7 1.1 %fusion.12 = f32[512,1,64]{2,0,1:T(8,128)S(1)} fusion(f32[64]{0:T(128)} %param.18, f32[512]{0:T(512)S(1)} %add_rsqrt_fusion.1, bf16[512,256]{1,0:T(8,128)(2,1)} %param.15, s32[]{:T(128)S(6)} %select_n.59), kind=kLoop, calls=%fused_computation.20 | loop fusion | flops 98304 | bytes 198916 | tf_op jit(solution)/shard_map/mul | solution.py:17
  6.8 2.4 %fusion.18 = (bf16[512,1,16]{2,0,1:T(8,128)(2,1)S(1)}, bf16[512,1,16]{2,0,1:T(8,128)(2,1)S(1)}, bf16[512,1,16]{2,0,1:T(8,128)(2,1)S(1)}, bf16[512,1,16]{2,0,1:T(8,128)(2,1)S(1)}) fusion(f32[512,1,64]{2,0,1:T(8,128)S(1)} %fusion.12, f32[512]{0:T(512)S(1)} %get-tuple-element.20, f32[16]{0:T(128)S(1)} %multiply_power_fusion, f32[512]{0:T(512)S(1)} %get-tuple-element.21), kind=kLoop, calls=%fused_computation.26 | loop fusion | flops 147456 | bytes 200768 | tf_op jit(solution)/shard_map/convert.1
  9.2 0.2 maximum_bitcast_fusion
  9.4 0.8 pad_maximum_fusion.pair_ref
  10.2 1.1 %copy.23 = bf16[512,256]{0,1:T(8,128)(2,1)S(1)} copy(bf16[512,256]{1,0:T(8,128)(2,1)} %param.14) | data formatting | bytes 524288 | tf_op args[0]
  11.3 0.1 fusion
  11.4 0.0 copy-done.1
  11.4 0.1 fusion.1
  11.5 0.1 subtract_convert_fusion.1
  11.6 0.3 copy.24
  11.9 0.9 %concatenate.15.q_ref = bf16[2048,128]{1,0:T(8,128)(2,1)} pad(bf16[2048,64]{1,0:T(8,128)(2,1)S(1)} %bitcast.19, bf16[]{:T(256)} %constant.91.clone.1), padding=0_0x0_64 | pad | bytes 786434 | tf_op jit(solution)/shard_map/concatenate | solution.py:370
  12.8 72.5 %shard_map.149 = (bf16[128,2048]{1,0:T(8,128)(2,1)}, bf16[128,512]{1,0:T(8,128)(2,1)}) custom-call(bf16[2048,128]{1,0:T(8,128)(2,1)} %concatenate.15.q_ref, bf16[512,128]{1,0:T(8,128)(2,1)} %pad_maximum_fusion.pair_ref, bf16[128,2048]{1,0:T(8,128)(2,1)} %x_ref.1, s32[128,2]{1,0:T(8,128)} %copy.27.route_ref, f32[128,2]{1,0:T(8,128)} %copy.28.logit_ref, ...), custom_call_target="tpu_custom_call" | custom-call | tf_op jit(solution)/shard_map/pallas_call | solution.py:392
  85.3 1.9 %copy.31 = bf16[128,2048]{1,0:T(8,128)(2,1)} copy(bf16[128,2048]{1,0:T(8,128)(2,1)} %get-tuple-element.26) | data formatting | bytes 1048576
  87.2 1.6 %copy.32 = bf16[128,512]{1,0:T(8,128)(2,1)} copy(bf16[128,512]{1,0:T(8,128)(2,1)} %get-tuple-element.27) | data formatting | bytes 262144
  (6 shorter events, 0.1 us)
Async XLA Ops:
  0.6 4.7 %copy-start = (bf16[512,256]{1,0:T(8,128)(2,1)S(1)}, bf16[512,256]{1,0:T(8,128)(2,1)}, u32[]{:S(2)}) copy-start(bf16[512,256]{1,0:T(8,128)(2,1)} %param.16) | copy-start | bytes 786436
  0.6 10.7 %copy-start.1 = (f32[64]{0:T(128)S(1)}, f32[64]{0:T(128)}, u32[]{:S(2)}) copy-start(f32[64]{0:T(128)} %param.17) | copy-start | bytes 772
where the time goes:
time: 90 us; the launch traced here: 88.7 us
  Pallas kernels  72.5 us (81%)
  local copies, waits for them, and re-layouts  8.64 us (10%)
  other arithmetic  6.86 us (8%)
    pallas_call x1, Pallas kernels, per_device(): pl.pallas_call(functools.partial(kernel, (n_ep, n_tp, heads, cap)), out_s...  72.5 us
    unnamed x9, local copies, waits for them, and re-layouts  7.36 us
    another operation x2, other arithmetic  2.48 us

commit v1 on v0

--- a/solution.py
+++ b/solution.py
@@ -2,6 +2,7 @@
 
 import jax
 import jax.numpy as jnp
+import numpy as np
 from jax import lax
 from jax.experimental import pallas as pl
 from jax.experimental.pallas import tpu as pltpu
@@ -13,53 +14,36 @@
 MESH = pl.DeviceIdType.MESH
 
 
-def head_norm(values, gain):
-    return values * lax.rsqrt(jnp.mean(values * values, axis=-1, keepdims=True) + EPSILON) * gain
-
-
-def rotate_half(values, angles):
-    quarter = angles.shape[-1]
-    first_part = values[..., :quarter]
-    second_part = values[..., quarter:]
-    cosine = jnp.cos(angles)[:, None, :]
-    sine_part = jnp.sin(angles)[:, None, :]
-    return jnp.concatenate(
-        [
-            first_part * cosine - second_part * sine_part,
-            second_part * cosine + first_part * sine_part,
-        ],
-        axis=-1,
-    )
-
-
-def grid_rotary(values, offset):
-    row_count = values.shape[0]
-    head_width = values.shape[-1]
-    quarter = head_width // 4
-    half_width = head_width // 2
-    position = offset + jnp.arange(row_count, dtype=jnp.int32)
-    grid_row = (position // GRID_W).astype(jnp.float32)
-    grid_col = (position % GRID_W).astype(jnp.float32)
-    inverse = ROPE_BASE ** (-jnp.arange(quarter, dtype=jnp.float32) / quarter)
-    return jnp.concatenate(
-        [
-            rotate_half(values[..., :half_width], grid_row[:, None] * inverse[None, :]),
-            rotate_half(values[..., half_width:], grid_col[:, None] * inverse[None, :]),
-        ],
-        axis=-1,
-    )
+def turn_tables(positions, rows_of_grid, quarter):
+    inverse = ROPE_BASE ** (-np.arange(quarter, dtype=np.float32) / np.float32(quarter))
+    inverse = inverse.astype(np.float32)
+
+    def table(count, first_half):
+        angles = (np.arange(count, dtype=np.float32)[:, None] * inverse[None, :]).astype(np.float64)
+        cos, sin = np.cos(angles), np.sin(angles)
+        none = np.zeros_like(cos)
+        cos = np.concatenate([cos, cos, none, none] if first_half else [none, none, cos, cos], axis=1)
+        sin = np.concatenate([-sin, sin, none, none] if first_half else [none, none, -sin, sin], axis=1)
+        return np.concatenate([cos, cos], axis=1), np.concatenate([sin, sin], axis=1)
+
+    grid_rows = positions // rows_of_grid
+    by_row = table(grid_rows, True)
+    by_col = table(rows_of_grid, False)
+    return [jnp.asarray(part, jnp.float32) for part in by_row + by_col]
 
 
 def kernel(
     dims,
-    q_ref, pair_ref, x_ref, route_ref, logit_ref, pre_ref, ids_ref, wout_ref, gain_ref, wg_hbm, wu_hbm, wd_hbm,
+    route_ref, logit_ref, pre_ref, gain_ref, qg_ref, kg_ref, crow_ref, srow_ref, ccol_ref, scol_ref,
+    q_hbm, k_hbm, v_hbm, x_hbm, wout_hbm, wg_hbm, wu_hbm, wd_hbm,
     attn_ref, moe_ref,
+    q_in, k_in, v_in, x_ref, wout_ref, q_ref, pair_ref, placed_ref,
     outgo_ref, mixw_ref, wg, wu, wd, kvbuf, vx, kt, acc, arrived, hidden,
     pa, pa_in, pa_red, pa_in2, pm, pm_in, pm_red, pm_in2, summed, ret,
-    w_sem, loc_sem, kv_s, kv_r, disp_s, disp_r, rel_s, rel_r, fwd_s,
+    in_sem, w_sem, loc_sem, kv_s, kv_r, disp_s, disp_r, rel_s, rel_r, fwd_s,
     a1_s, a1_r, a2_s, a2_r, m1_s, m1_r, m2_s, m2_r, ret_s, ret_r,
 ):
-    n_ep, n_tp, heads, cap = dims
+    n_ep, n_tp, heads, cap, repeat = dims
     ny = n_tp // 2
     ep = lax.axis_index("ep")
     tp = lax.axis_index("tp")
@@ -92,6 +76,19 @@
     def slot_rows(e):
         return pl.ds(pl.multiple_of(e * cap, cap), cap)
 
+    head = qg_ref.shape[1]
+    lane_count = 2 * head
+    kv_index = tp * heads // repeat
+    kv_lanes = pl.ds(pl.multiple_of((kv_index // 2) * lane_count, lane_count), lane_count)
+    ins = [
+        pltpu.make_async_copy(src, dst, in_sem.at[i])
+        for i, (src, dst) in enumerate((
+            (x_hbm, x_ref), (k_hbm.at[:, kv_lanes], k_in), (v_hbm.at[:, kv_lanes], v_in),
+            (q_hbm, q_in), (wout_hbm, wout_ref),
+        ))
+    ]
+    for copy in ins[:4]:
+        copy.start()
     loads = [
         pltpu.make_async_copy(src, dst, w_sem.at[i])
         for i, (src, dst) in enumerate(((wg_hbm, wg), (wu_hbm, wu), (wd_hbm, wd)))
@@ -103,34 +100,73 @@
         pl.semaphore_signal(barrier, inc=1, device_id=(ep, same_core(d)), device_id_type=MESH)
     pl.semaphore_signal(barrier, inc=1, device_id=(ep, partner), device_id_type=MESH)
 
-    x = x_ref[...].astype(jnp.float32)
+    bf16, f32 = jnp.bfloat16, jnp.float32
+    top, tokens = logit_ref.shape
+    logits = logit_ref[...]
+    power = jnp.exp(logits - jnp.max(logits, axis=0, keepdims=True))
+    chance = power / jnp.sum(power, axis=0, keepdims=True)
+    expert = lax.broadcasted_iota(jnp.int32, (n_ep, tokens), 0)
+    named = jnp.zeros((n_ep, tokens), f32)
+    share = jnp.zeros((n_ep, tokens), f32)
+    for j in range(top):
+        hit = route_ref[j : j + 1, :] == expert
+        named = jnp.where(hit, 1.0, named)
+        share = jnp.where(hit, chance[j : j + 1, :], share)
+    above = lax.broadcasted_iota(jnp.int32, (tokens, tokens), 0) < lax.broadcasted_iota(
+        jnp.int32, (tokens, tokens), 1
+    )
+    rank = jnp.dot(named, jnp.where(above, 1.0, 0.0), preferred_element_type=f32)
+    rank = jnp.where(named > 0.0, rank, -1.0)
+    place = lax.broadcasted_iota(jnp.int32, (cap, tokens), 0).astype(f32)
+    for e in range(n_ep):
+        there = rank[e : e + 1, :] == place
+        placed_ref[e * cap : (e + 1) * cap, :] = jnp.where(there, 1.0, 0.0).astype(bf16)
+        mixw_ref[e * cap : (e + 1) * cap, :] = jnp.where(there, share[e : e + 1, :], 0.0)
+
+    ins[0].wait()
+    x = x_ref[...].astype(f32)
     scale = lax.rsqrt(jnp.mean(x * x, axis=-1, keepdims=True) + EPSILON)
     mine = pl.ds(pl.multiple_of(tp * dq, dq), dq)
-    normed = (x_ref[:, mine].astype(jnp.float32) * scale * pre_ref[:, mine]).astype(jnp.bfloat16)
-    logits = logit_ref[...]
-    top = logits.shape[1]
-    tokens = logits.shape[0]
-    power = jnp.exp(logits - jnp.max(logits, axis=1, keepdims=True))
-    chance = power / jnp.sum(power, axis=1, keepdims=True)
-    named = jnp.zeros((tokens, slots), jnp.float32)
-    share = jnp.zeros((tokens, slots), jnp.float32)
-    for j in range(top):
-        hit = route_ref[:, j : j + 1] == ids_ref[0:1, :]
-        named = jnp.where(hit, 1.0, named)
-        share = jnp.where(hit, chance[:, j : j + 1], share)
-    below = lax.broadcasted_iota(jnp.int32, (tokens, tokens), 1) < lax.broadcasted_iota(
-        jnp.int32, (tokens, tokens), 0
+    normed = (x_ref[:, mine].astype(f32) * scale * pre_ref[:, mine]).astype(bf16)
+    outgo_ref[...] = jnp.dot(placed_ref[...], normed, preferred_element_type=f32).astype(bf16)
+
+    lane = lax.broadcasted_iota(jnp.int32, (GRID_W, lane_count), 1)
+    first = lane < head
+    ahead = lax.rem(lane, head // 2) < head // 4
+    joined = lax.broadcasted_iota(jnp.int32, (lane_count, lane_count), 0) // head == (
+        lax.broadcasted_iota(jnp.int32, (lane_count, lane_count), 1) // head
     )
-    rank = jnp.dot(
-        jnp.where(below, 1.0, 0.0).astype(jnp.bfloat16), named.astype(jnp.bfloat16),
-        preferred_element_type=jnp.float32,
-    )
-    placed = jnp.where(rank == ids_ref[1:2, :].astype(jnp.float32), named, 0.0)
-    mixw_ref[...] = placed * share
-    outgo_ref[...] = lax.dot_general(
-        placed.astype(jnp.bfloat16), normed, (((0,), (0,)), ((), ())),
-        preferred_element_type=jnp.float32,
-    ).astype(jnp.bfloat16)
+    joined = jnp.where(joined, 1.0, 0.0).astype(bf16)
+    blocks = rows_kv // GRID_W
+
+    def turned(values, gain, b):
+        square = values * values
+        high = square.astype(bf16)
+        low = (square - high.astype(f32)).astype(bf16)
+        total = jnp.dot(high, joined, preferred_element_type=f32) + jnp.dot(
+            low, joined, preferred_element_type=f32
+        )
+        values = values * lax.rsqrt(total * (1.0 / head) + EPSILON) * gain
+        other = jnp.where(
+            ahead,
+            pltpu.roll(values, lane_count - head // 4, 1),
+            pltpu.roll(values, head // 4, 1),
+        )
+        at = pl.ds(ep * blocks + b, 1)
+        return values * (crow_ref[at, :] + ccol_ref[...]) + other * (srow_ref[at, :] + scol_ref[...])
+
+    k_gain = jnp.concatenate([kg_ref[...], kg_ref[...]], axis=1)
+    q_gain = jnp.concatenate([qg_ref[...], qg_ref[...]], axis=1)
+    odd = lax.rem(kv_index, 2)
+    ins[1].wait()
+    ins[2].wait()
+    for b in range(blocks):
+        at = slice(b * GRID_W, (b + 1) * GRID_W)
+        keys = turned(k_in[at, :].astype(f32), k_gain, b)
+        keys = jnp.where(odd == 1, pltpu.roll(keys, head, 1), keys)
+        values = v_in[at, :].astype(f32)
+        values = jnp.where(odd == 1, values, pltpu.roll(values, head, 1))
+        pair_ref[at, :] = jnp.where(first, keys, values).astype(bf16)
     own = pltpu.make_async_copy(
         outgo_ref.at[slot_rows(ep)], arrived.at[tp, slot_rows(ep)], loc_sem.at[0]
     )
@@ -166,6 +202,22 @@
         kv_direct(d).start()
     for copy in loads:
         copy.start()
+    ins[4].start()
+
+    ins[3].wait()
+    for g in range(max(1, heads // 2)):
+        for b in range(blocks):
+            at = slice(b * GRID_W, (b + 1) * GRID_W)
+            if heads == 1:
+                values = q_in[at, :].astype(f32)
+                values = jnp.concatenate([values, jnp.zeros_like(values)], axis=1)
+            else:
+                values = q_in[at, g * lane_count : (g + 1) * lane_count].astype(f32)
+            values = turned(values, q_gain, b) * (head ** (-0.5))
+            for h in range(min(2, heads)):
+                part = values if h == 0 else pltpu.roll(values, head, 1)
+                row_at = (2 * g + h) * rows_kv + b * GRID_W
+                q_ref[row_at : row_at + GRID_W, :] = jnp.where(first, part, 0.0).astype(bf16)
 
     q_rows = q_ref.shape[0]
     tile = min(512, q_rows // 2)
@@ -228,7 +280,7 @@
         cross[d].start()
     lax.fori_loop(late, nz, later, 0)
 
-    outs = []
+    ins[4].wait()
     tokens = q_rows // heads
     half = acc.shape[1] // 2
     for j in range(n_tp):
@@ -335,9 +387,10 @@
     mixw = mixw_ref[...]
     high = mixw.astype(jnp.bfloat16)
     low = (mixw - high.astype(jnp.float32)).astype(jnp.bfloat16)
+    over = (((0,), (0,)), ((), ()))
     moe_ref[...] = (
-        jnp.dot(high, ret[...], preferred_element_type=jnp.float32)
-        + jnp.dot(low, ret[...], preferred_element_type=jnp.float32)
+        lax.dot_general(high, ret[...], over, preferred_element_type=jnp.float32)
+        + lax.dot_general(low, ret[...], over, preferred_element_type=jnp.float32)
     ).astype(jnp.bfloat16)
 
     for copy in [kv_mate] + disp + relay + cross + [a1] + a2 + [m1] + m2 + back:
@@ -363,17 +416,7 @@
     kv_count = k_in.shape[1] // head
     repeat = heads * n_tp // kv_count
     ny = n_tp // 2
-    offset = lax.axis_index("ep") * rows
-    queries = head_norm(q_in.astype(jnp.float32).reshape(rows, heads, head), q_gain)
-    queries = grid_rotary(queries, offset).astype(bf16) * jnp.asarray(head ** (-0.5), bf16)
-    queries = jnp.transpose(queries, (1, 0, 2)).reshape(heads * rows, head)
-    queries = jnp.concatenate([queries, jnp.zeros_like(queries)], axis=1)
-    kv_index = lax.axis_index("tp") * heads // repeat
-    keys = lax.dynamic_slice_in_dim(k_in, kv_index * head, head, 1)
-    values = lax.dynamic_slice_in_dim(v_in, kv_index * head, head, 1)
-    keys = head_norm(keys.astype(jnp.float32)[:, None, :], k_gain)
-    keys = grid_rotary(keys, offset)[:, 0, :].astype(bf16)
-    paired = jnp.concatenate([keys, values], axis=1)
+    grid_rows = turn_tables(n_ep * rows, GRID_W, head // 4)
 
     tokens, top = routes.shape
     width = moe_in.shape[1]
@@ -381,8 +424,6 @@
     need = max(2, 3 * top * tokens // (2 * n_ep))
     cap = -(-need // 16) * 16
     slots = n_ep * cap
-    slot = jnp.arange(slots, dtype=jnp.int32)
-    ids = jnp.stack([slot // cap, slot % cap])
 
     piece = rows // n_tp
     ff = w_gate.shape[2]
@@ -390,16 +431,24 @@
     vmem = pl.BlockSpec(memory_space=pltpu.VMEM)
     hbm = pl.BlockSpec(memory_space=pl.ANY)
     return pl.pallas_call(
-        functools.partial(kernel, (n_ep, n_tp, heads, cap)),
+        functools.partial(kernel, (n_ep, n_tp, heads, cap, repeat)),
         out_shape=(
             jax.ShapeDtypeStruct((piece, width), bf16),
             jax.ShapeDtypeStruct((tokens, dq), bf16),
         ),
-        in_specs=[vmem] * 9 + [hbm] * 3,
+        in_specs=[vmem] * 10 + [hbm] * 8,
         out_specs=(vmem, vmem),
         scratch_shapes=[
+            pltpu.VMEM((rows, heads * head), bf16),
+            pltpu.VMEM((rows, 2 * head), bf16),
+            pltpu.VMEM((rows, 2 * head), bf16),
+            pltpu.VMEM((tokens, width), bf16),
+            pltpu.VMEM((heads * head, width), bf16),
+            pltpu.VMEM((heads * rows, 2 * head), bf16),
+            pltpu.VMEM((rows, 2 * head), bf16),
+            pltpu.VMEM((slots, tokens), bf16),
             pltpu.VMEM((slots, dq), bf16),
-            pltpu.VMEM((tokens, slots), jnp.float32),
+            pltpu.VMEM((slots, tokens), jnp.float32),
             pltpu.VMEM((width, ff), bf16),
             pltpu.VMEM((width, ff), bf16),
             pltpu.VMEM((ff, width), bf16),
@@ -419,7 +468,7 @@
             pltpu.VMEM((ny, slots, dq), bf16),
             pltpu.VMEM((slots, dq), bf16),
             pltpu.VMEM((slots, dq), bf16),
-            dma((3,)), dma((2,)),
+            dma((5,)), dma((3,)), dma((2,)),
             dma((n_ep,)), dma((n_ep,)), dma((n_ep,)), dma((n_ep,)),
             dma((ny,)), dma((2 * ny,)), dma((ny,)),
             dma((1,)), dma((1,)), dma((ny,)), dma((ny,)),
@@ -429,7 +478,10 @@
         compiler_params=pltpu.CompilerParams(
             collective_id=0, has_side_effects=True, vmem_limit_bytes=60 * 1024 * 1024
         ),
-    )(queries, paired, moe_in, routes, route_logits, pre_gain[None, :], ids, w_out, post_gain[None, :], w_gate[0], w_up[0], w_down[0])
+    )(
+        routes.T, route_logits.T, pre_gain[None, :], post_gain[None, :], q_gain[None, :], k_gain[None, :], *grid_rows,
+        q_in, k_in, v_in, moe_in, w_out, w_gate[0], w_up[0], w_down[0],
+    )
 
 
 def solution(mesh):

time: 90 us -> 77.2 us (0.86)
  other arithmetic: 6.86 us -> 0 us
  local copies, waits for them, and re-layouts: 8.64 us -> 3.45 us
    unnamed x9 -> x2, local copies, waits for them, and re-layouts: 7.36 us -> 3.45 us
    another operation x3 -> x0, other arithmetic: 3.06 us -> none
    reduce_sum x2 -> x0, other arithmetic: 1.24 us -> none  [head_norm(): jnp.mean(values * values, axis=-1, keepdims=True) + EPSILON]
    mul x2 -> x0, other arithmetic: 1.2 us -> none  [head_norm(): values * lax.rsqrt(jnp.mean(values * values, axis=-1, keepdims=True) + EP...]
    concatenate x1 -> x0, local copies, waits for them, and re-layouts: 0.9 us -> none  [per_device(): queries = jnp.concatenate([queries, jnp.zeros_like(queries)], axis=1)]
where the time goes in v1:
time: 77.2 us; the launch traced here: 76 us
  Pallas kernels  72 us (93%)
  local copies, waits for them, and re-layouts  3.45 us (4%)
    pallas_call x1, Pallas kernels, per_device(): pl.pallas_call(functools.partial(kernel, (n_ep, n_tp, heads, cap, repeat)...  72 us
    unnamed x2, local copies, waits for them, and re-layouts  3.45 us

profile of v1, /device:TPU:0, one launch (start us, length us, event | category | flops | bytes accessed | tf_op | source)
XLA Modules:
  0.0 76.0 jit_solution(7486570708195396576)
XLA Ops:
  0.6 72.0 %shard_map.185 = (bf16[128,2048]{1,0:T(8,128)(2,1)}, bf16[128,512]{1,0:T(8,128)(2,1)}) custom-call(s32[2,128]{1,0:T(2,128)} %bitcast.14, f32[2,128]{1,0:T(2,128)} %bitcast.15, f32[1,2048]{1,0:T(1,128)} %bitcast.12, f32[1,2048]{1,0:T(1,128)} %bitcast.13, f32[1,64]{1,0:T(1,128)} %bitcast.16, f32[1,64]{1,0:T(1,128)} %bitcast.17, ...), custom_call_target="tpu_custom_call" | custom-call | tf_op jit(solution)/shard_map/pallas_call | solution.py:433
  72.6 1.9 %copy.22 = bf16[128,2048]{1,0:T(8,128)(2,1)} copy(bf16[128,2048]{1,0:T(8,128)(2,1)} %get-tuple-element.4) | data formatting | bytes 1048576
  74.5 1.6 %copy.23 = bf16[128,512]{1,0:T(8,128)(2,1)} copy(bf16[128,512]{1,0:T(8,128)(2,1)} %get-tuple-element.5) | data formatting | bytes 262144

commit v2 on v1

v2 whole, which is shorter than its diff:
```python
import functools

import jax
import jax.numpy as jnp
import numpy as np
from jax import lax
from jax.experimental import pallas as pl
from jax.experimental.pallas import tpu as pltpu
from jax.sharding import PartitionSpec as P

GRID_W = 128
EPSILON = 1e-06
ROPE_BASE = 10000.0
MESH = pl.DeviceIdType.MESH


def turn_tables(positions, rows_of_grid, quarter):
    inverse = ROPE_BASE ** (-np.arange(quarter, dtype=np.float32) / np.float32(quarter))
    inverse = inverse.astype(np.float32)

    def table(count, first_half):
        angles = (np.arange(count, dtype=np.float32)[:, None] * inverse[None, :]).astype(np.float64)
        cos, sin = np.cos(angles), np.sin(angles)
        none = np.zeros_like(cos)
        cos = np.concatenate([cos, cos, none, none] if first_half else [none, none, cos, cos], axis=1)
        sin = np.concatenate([-sin, sin, none, none] if first_half else [none, none, -sin, sin], axis=1)
        return np.concatenate([cos, cos], axis=1), np.concatenate([sin, sin], axis=1)

    grid_rows = positions // rows_of_grid
    by_row = table(grid_rows, True)
    by_col = table(rows_of_grid, False)
    return [jnp.asarray(part, jnp.float32) for part in by_row + by_col]


def kernel(
    dims,
    route_ref, logit_ref, pre_ref, gain_ref, qg_ref, kg_ref, crow_ref, srow_ref, ccol_ref, scol_ref,
    q_hbm, k_hbm, v_hbm, x_hbm, wout_hbm, wg_hbm, wu_hbm, wd_hbm,
    attn_ref, moe_ref,
    q_in, k_in, v_in, x_ref, wout_ref, q_ref, placed_ref,
    outgo_ref, mixw_ref, wg, wu, wd, kvbuf, vx, kt, acc, arrived, hidden,
    pa, pa_in, pa_red, pa_in2, pm, pm_in, pm_red, pm_in2, summed, ret,
    in_sem, w_sem, kz_s, kz_r, kx_s, kx_r, disp_s, disp_r, rel_s, rel_r, c0_s, c0_r, cy_s, cy_r,
    a1_s, a1_r, a2_s, a2_r, m1_s, m1_r, m2_s, m2_r, ret_s, ret_r,
):
    n_ep, n_tp, heads, cap, repeat = dims
    ny = n_tp // 2
    nz = n_ep // 2
    ep = lax.axis_index("ep")
    tp = lax.axis_index("tp")
    core = lax.rem(tp, 2)
    row = lax.div(tp, 2)
    partner = row * 2 + 1 - core
    side = lax.rem(ep, 2)
    col = lax.div(ep, 2)
    mate = col * 2 + 1 - side
    rows_kv = k_in.shape[0]
    dq = outgo_ref.shape[1]
    slots = outgo_ref.shape[0]
    piece = attn_ref.shape[0]
    bf16, f32 = jnp.bfloat16, jnp.float32

    def remote(src, dst, ss, rs, e, t):
        return pltpu.make_async_remote_copy(
            src_ref=src, dst_ref=dst, send_sem=ss, recv_sem=rs,
            device_id=(e, t), device_id_type=MESH,
        )

    def wait(name, copy):
        with jax.named_scope(name):
            copy.wait_recv()

    def ep_at(d):
        return lax.rem(ep + d, n_ep)

    def flip(d):
        other = ep
        for bit in range(n_ep.bit_length() - 1):
            if (d >> bit) % 2:
                other = other + (1 << bit) * (1 - 2 * lax.rem(lax.div(ep, 1 << bit), 2))
        return other

    def same_core(d):
        return lax.rem(row + d, ny) * 2 + core

    def row_from(d):
        return lax.rem(row - d + ny, ny)

    def slot_rows(e):
        return pl.ds(pl.multiple_of(e * cap, cap), cap)

    def lanes_of(t):
        return pl.ds(pl.multiple_of(t * dq, dq), dq)

    quarter = n_ep // 4
    near = list(range(quarter - 1, -1, -1))
    groups = [
        list(range(2 * quarter, 3 * quarter)) + near,
        list(range(3 * quarter, 4 * quarter)) + list(range(quarter, 2 * quarter)),
    ]
    order = groups[0] + groups[1]
    chunk = slots // 2
    part = chunk // 2

    def held(d):
        return pl.ds(order.index(d) * cap, cap)

    head = qg_ref.shape[1]
    lane_count = 2 * head
    kv_index = lax.div(tp * heads, repeat)
    kv_lanes = pl.ds(pl.multiple_of(lax.div(kv_index, 2) * lane_count, lane_count), lane_count)
    ins = [
        pltpu.make_async_copy(src, dst, in_sem.at[i])
        for i, (src, dst) in enumerate((
            (x_hbm, x_ref), (k_hbm.at[:, kv_lanes], k_in), (v_hbm.at[:, kv_lanes], v_in),
            (q_hbm, q_in), (wout_hbm, wout_ref),
        ))
    ]
    for copy in ins[:4]:
        copy.start()
    loads = [
        pltpu.make_async_copy(src, dst, w_sem.at[i])
        for i, (src, dst) in enumerate(((wg_hbm, wg), (wu_hbm, wu), (wd_hbm, wd)))
    ]
    barrier = pltpu.get_barrier_semaphore()
    for d in range(1, n_ep):
        pl.semaphore_signal(barrier, inc=1, device_id=(ep_at(d), tp), device_id_type=MESH)
    for d in range(1, ny):
        pl.semaphore_signal(barrier, inc=1, device_id=(ep, same_core(d)), device_id_type=MESH)
    pl.semaphore_signal(barrier, inc=1, device_id=(ep, partner), device_id_type=MESH)

    top, tokens = logit_ref.shape
    logits = logit_ref[...]
    power = jnp.exp(logits - jnp.max(logits, axis=0, keepdims=True))
    chance = power / jnp.sum(power, axis=0, keepdims=True)
    expert = lax.broadcasted_iota(jnp.int32, (n_ep, tokens), 0)
    named = jnp.zeros((n_ep, tokens), f32)
    share = jnp.zeros((n_ep, tokens), f32)
    for j in range(top):
        hit = route_ref[j : j + 1, :] == expert
        named = jnp.where(hit, 1.0, named)
        share = jnp.where(hit, chance[j : j + 1, :], share)
    above = lax.broadcasted_iota(jnp.int32, (tokens, tokens), 0) < lax.broadcasted_iota(
        jnp.int32, (tokens, tokens), 1
    )
    rank = jnp.dot(named, jnp.where(above, 1.0, 0.0), preferred_element_type=f32)
    rank = jnp.where(named > 0.0, rank, -1.0)
    place = lax.broadcasted_iota(jnp.int32, (cap, tokens), 0).astype(f32)
    for e in range(n_ep):
        there = rank[e : e + 1, :] == place
        placed_ref[e * cap : (e + 1) * cap, :] = jnp.where(there, 1.0, 0.0).astype(bf16)
        mixw_ref[e * cap : (e + 1) * cap, :] = jnp.where(there, share[e : e + 1, :], 0.0)

    ins[0].wait()
    x = x_ref[...].astype(f32)
    scale = lax.rsqrt(jnp.mean(x * x, axis=-1, keepdims=True) + EPSILON)
    mine = pl.ds(pl.multiple_of(tp * dq, dq), dq)
    normed = (x_ref[:, mine].astype(f32) * scale * pre_ref[:, mine]).astype(bf16)
    outgo_ref[...] = jnp.dot(placed_ref[...], normed, preferred_element_type=f32).astype(bf16)

    lane = lax.broadcasted_iota(jnp.int32, (GRID_W, lane_count), 1)
    first = lane < head
    ahead = lax.rem(lane, head // 2) < head // 4
    joined = lax.broadcasted_iota(jnp.int32, (lane_count, lane_count), 0) // head == (
        lax.broadcasted_iota(jnp.int32, (lane_count, lane_count), 1) // head
    )
    joined = jnp.where(joined, 1.0, 0.0).astype(bf16)
    blocks = rows_kv // GRID_W

    def turned(values, gain, b):
        square = values * values
        high = square.astype(bf16)
        low = (square - high.astype(f32)).astype(bf16)
        total = jnp.dot(high, joined, preferred_element_type=f32) + jnp.dot(
            low, joined, preferred_element_type=f32
        )
        values = values * lax.rsqrt(total * (1.0 / head) + EPSILON) * gain
        other = jnp.where(
            ahead,
            pltpu.roll(values, lane_count - head // 4, 1),
            pltpu.roll(values, head // 4, 1),
        )
        at = pl.ds(ep * blocks + b, 1)
        return values * (crow_ref[at, :] + ccol_ref[...]) + other * (srow_ref[at, :] + scol_ref[...])

    k_gain = jnp.concatenate([kg_ref[...], kg_ref[...]], axis=1)
    q_gain = jnp.concatenate([qg_ref[...], qg_ref[...]], axis=1)
    odd = lax.rem(kv_index, 2)
    ins[1].wait()
    ins[2].wait()
    for b in range(blocks):
        at = slice(b * GRID_W, (b + 1) * GRID_W)
        keys = turned(k_in[at, :].astype(f32), k_gain, b)
        keys = jnp.where(odd == 1, pltpu.roll(keys, head, 1), keys)
        values = v_in[at, :].astype(f32)
        values = jnp.where(odd == 1, values, pltpu.roll(values, head, 1))
        kvbuf[ep, at, :] = jnp.where(first, keys, values).astype(bf16)
    with jax.named_scope("barrier"):
        pl.semaphore_wait(barrier, n_ep - 1 + ny - 1 + 1)

    disp = {
        d: remote(outgo_ref.at[slot_rows(flip(d))], arrived.at[held(d), lanes_of(tp)],
                  disp_s.at[d], disp_r.at[d], flip(d), tp)
        for d in range(1, n_ep)
    }

    def kv_line(b, target, sem):
        block = kvbuf.at[b * 2 + side]
        return remote(block, block, kz_s.at[sem], kz_r.at[b], target * 2 + side, tp)

    def kv_pass(b):
        block = kvbuf.at[b * 2 + side]
        return remote(block, block, kx_s.at[b], kx_r.at[b], mate, tp)

    has_next = col < nz - 1
    has_prev = col > 0

    kv_pass(col).start()
    for d in groups[0]:
        if d:
            disp[d].start()

    @pl.when(has_next)
    def _():
        kv_line(col, col + 1, col).start()

    @pl.when(has_prev)
    def _():
        kv_line(col, col - 1, nz).start()

    for d in groups[1]:
        disp[d].start()
    for copy in loads:
        copy.start()
    ins[4].start()

    ins[3].wait()
    for g in range(max(1, heads // 2)):
        for b in range(blocks):
            at = slice(b * GRID_W, (b + 1) * GRID_W)
            if heads == 1:
                values = q_in[at, :].astype(f32)
                values = jnp.concatenate([values, jnp.zeros_like(values)], axis=1)
            else:
                values = q_in[at, g * lane_count : (g + 1) * lane_count].astype(f32)
            values = turned(values, q_gain, b) * (head ** (-0.5))
            for h in range(min(2, heads)):
                one = values if h == 0 else pltpu.roll(values, head, 1)
                one = jnp.where(first, one, 0.0).astype(bf16)
                for i in range(max(1, GRID_W // piece)):
                    size = min(piece, GRID_W)
                    token = b * GRID_W + i * size
                    row_at = (token // piece * heads + 2 * g + h) * piece + token % piece
                    q_ref[row_at : row_at + size, :] = one[i * size : (i + 1) * size, :]

    mine_rows = placed_ref[slot_rows(ep), :]
    for q in range(n_tp):
        at = slice(q * dq, (q + 1) * dq)
        full = (x_ref[:, at].astype(f32) * scale * pre_ref[:, at]).astype(bf16)
        arrived[held(0), at] = jnp.dot(mine_rows, full, preferred_element_type=f32).astype(bf16)

    q_rows = q_ref.shape[0]
    tile = min(512, heads * piece)

    def prepare(e, slot):
        keys = kvbuf[e]
        lanes = lax.broadcasted_iota(jnp.int32, keys.shape, 1)
        kt[slot] = keys.T
        vx[slot] = jnp.where(lanes < keys.shape[1] // 2, jnp.ones_like(keys), keys)

    def attend_rows(i, slot, fresh):
        for sub in range(2):
            at = pl.ds(pl.multiple_of(i * 2 * tile + sub * tile, tile), tile)
            scores = jnp.dot(q_ref[at, :], kt[slot], preferred_element_type=f32)
            weights = jnp.exp(scores).astype(bf16)
            term = jnp.dot(weights, vx[slot], preferred_element_type=f32)
            if fresh:
                acc[at, :] = term
            else:
                acc[at, :] += term

    def attend(e, fresh):
        prepare(e, 0)

        def one(i, carry):
            attend_rows(i, 0, fresh)
            return carry

        lax.fori_loop(0, q_rows // (2 * tile), one, 0)

    shorter = jnp.minimum(col, nz - 1 - col)
    longer = jnp.where(col <= nz - 1 - col, 1, -1)

    def line_step(k):
        both = k < 2 * shorter
        way = jnp.where(both, 2 * lax.rem(k, 2) - 1, longer)
        far = jnp.where(both, lax.div(k, 2) + 1, k - shorter + 1)
        return col + way * far, col - way

    def line_one(k):
        b, target = line_step(k)
        wait("kv_line", kv_line(b, target, b))

        @pl.when(jnp.logical_and(target >= 0, target <= nz - 1))
        def _():
            kv_line(b, target, b).start()

        kv_pass(b).start()

    def line_take(k):
        both = k < 2 * shorter
        opening = jnp.logical_or(lax.rem(k, 2) == 0, jnp.logical_not(both))

        @pl.when(opening)
        def _():
            line_one(k)

        @pl.when(jnp.logical_and(opening, both))
        def _():
            line_one(k + 1)

    def line_block(k):
        return line_step(k)[0] * 2 + side

    def pass_block(k):
        b, _ = line_step(k)
        wait("kv_pass", kv_pass(b))
        return b * 2 + 1 - side

    def take(k, carry):
        line_take(k)
        attend(line_block(k), False)
        attend(pass_block(k), False)
        return carry

    def relay(d, dy):
        block = arrived.at[held(d), lanes_of(tp)]
        return remote(block, block, rel_s.at[d, dy], rel_r.at[d, dy], ep, same_core(dy))

    def foreign(c):
        count = len(groups[c]) - (1 if 0 in groups[c] else 0)
        return pl.ds(c * chunk, count * cap)

    def cross(c, dy):
        block = arrived.at[foreign(c), lanes_of(row_from(dy) * 2 + core)]
        if dy == 0:
            return remote(block, block, c0_s.at[c], c0_r.at[c], ep, partner)
        return remote(block, block, cy_s.at[c, dy], cy_r.at[c, dy], ep, partner)

    def relay_chunk(c):
        for d in groups[c]:
            if d:
                wait("disp", disp[d])
                for dy in range(1, ny):
                    relay(d, dy).start()
        cross(c, 0).start()

    def cross_chunk(c):
        for dy in range(1, ny):
            for d in groups[c]:
                if d:
                    wait("relay", relay(d, dy))
            cross(c, dy).start()

    ff = hidden.shape[1]
    step = min(256, ff)

    def m1(c):
        return remote(pm.at[c, 1 - core], pm_in.at[c], m1_s.at[c], m1_r.at[c], ep, partner)

    def m2(c, s, dy):
        at = pl.ds(s * part, part)
        return remote(pm_red.at[c, lax.rem(row + dy, ny), at], pm_in2.at[c, row, at],
                      m2_s.at[c, s, dy], m2_r.at[c, s, dy], ep, same_core(dy))

    def experts(c):
        for dy in range(ny):
            wait("cross", cross(c, dy))
        if c == 0:
            loads[0].wait()
            loads[1].wait()
        rows = slice(c * chunk, (c + 1) * chunk)

        def gated(i, carry):
            at = pl.ds(pl.multiple_of(i * step, step), step)
            x = arrived[rows, :]
            gate = jnp.dot(x, wg[:, at], preferred_element_type=f32)
            up = jnp.dot(x, wu[:, at], preferred_element_type=f32)
            hidden[rows, at] = (gate / (1.0 + jnp.exp(-gate)) * up).astype(bf16)
            return carry

        lax.fori_loop(0, ff // step, gated, 0)
        if c == 0:
            loads[2].wait()

        def down_for(which):
            def down(y, carry):
                cols = pl.ds(pl.multiple_of((y * 2 + which) * dq, dq), dq)
                pm[c, which, y] = jnp.dot(
                    hidden[rows, :], wd[:, cols], preferred_element_type=f32
                ).astype(bf16)
                return carry

            lax.fori_loop(0, ny, down, 0)

        down_for(1 - core)
        m1(c).start()
        down_for(core)

    def reduce_cores(c):
        wait("m1", m1(c))
        for y in range(ny):
            pm_red[c, y] = (pm[c, core, y].astype(f32) + pm_in[c, y].astype(f32)).astype(bf16)
        for s in range(2):
            for dy in range(1, ny):
                m2(c, s, dy).start()

    def back(d):
        return remote(summed.at[held(d)], ret.at[slot_rows(ep)], ret_s.at[d], ret_r.at[d], flip(d), tp)

    def send_back(c):
        for s in range(2):
            for dy in range(1, ny):
                wait("m2", m2(c, s, dy))
            at = slice(s * part, (s + 1) * part)
            total = pm_red[c, row, at].astype(f32)
            for dy in range(1, ny):
                total = total + pm_in2[c, row_from(dy), at].astype(f32)
            total = total.astype(bf16)
            rows_at = c * chunk + s * part
            summed[rows_at : rows_at + part, :] = total
            for d in order[rows_at // cap : (rows_at + part) // cap]:
                if d:
                    back(d).start()
                else:
                    low = order.index(0) * cap - rows_at
                    ret[slot_rows(ep), :] = total[low : low + cap, :]

    tall = heads * piece
    half = acc.shape[1] // 2

    def finish(target):
        for slot in range(2):
            for i in range(2 * tall // (2 * tile)):
                attend_rows(target * (tall // tile) + i, slot, False)
        sides = []
        for c in range(2):
            which = core if c else 1 - core
            pieces = []
            for h in range(heads):
                at = pl.ds(pl.multiple_of((target * 2 + which) * tall + h * piece, piece), piece)
                sums = acc[at, :]
                pieces.append((sums[:, half:] / sums[:, :half]).astype(bf16))
            sides.append(pieces[0] if heads == 1 else jnp.concatenate(pieces, axis=1))
        both = jnp.concatenate(sides, axis=0)
        return jnp.dot(both, wout_ref[...], preferred_element_type=f32)

    def a1(d):
        return remote(pa.at[d], pa_in.at[d], a1_s.at[d], a1_r.at[d], ep, partner)

    def a2(d):
        return remote(pa_red.at[d], pa_in2.at[d], a2_s.at[d], a2_r.at[d], ep, same_core(d))

    def finish_start(d):
        total = finish(lax.rem(row + d, ny)).astype(bf16)
        pa[d] = total[:piece]
        a1(d).start()
        pa_red[d] = total[piece:]

    def finish_end(d):
        wait("a1", a1(d))
        return pa_red[d].astype(f32) + pa_in[d].astype(f32)

    attend(ep, True)
    wait("kv_mate", kv_pass(col))
    attend(mate, False)
    relay_chunk(0)
    split = max(1, (nz - 1) // 2)
    line_take(0)
    attend(line_block(0), False)
    relay_chunk(1)
    attend(pass_block(0), False)
    lax.fori_loop(1, split, take, 0)
    cross_chunk(0)
    line_take(split)
    attend(line_block(split), False)
    with jax.named_scope("experts0"):
        experts(0)
    cross_chunk(1)
    attend(pass_block(split), False)
    reduce_cores(0)
    lax.fori_loop(split + 1, nz - 2, take, 0)
    line_take(nz - 2)
    prepare(line_block(nz - 2), 0)
    with jax.named_scope("experts1"):
        experts(1)
    send_back(0)
    prepare(pass_block(nz - 2), 1)
    ins[4].wait()
    reduce_cores(1)
    for d in range(1, ny):
        with jax.named_scope("finish_other"):
            finish_start(d)
    for d in range(1, ny):
        pa_red[d] = finish_end(d).astype(bf16)
        a2(d).start()
    send_back(1)
    with jax.named_scope("finish_own"):
        finish_start(0)
    mixed = finish_end(0).astype(bf16).astype(f32)
    for d in range(1, ny):
        wait("a2", a2(d))
        mixed = mixed + pa_in2[d].astype(f32)
    square = jnp.mean(mixed * mixed, axis=-1, keepdims=True)
    attn_ref[...] = (mixed * lax.rsqrt(square + EPSILON) * gain_ref[...]).astype(bf16)

    for d in range(1, n_ep):
        wait("back", back(d))
    mixw = mixw_ref[...]
    high = mixw.astype(bf16)
    low = (mixw - high.astype(f32)).astype(bf16)
    over = (((0,), (0,)), ((), ()))
    moe_ref[...] = (
        lax.dot_general(high, ret[...], over, preferred_element_type=f32)
        + lax.dot_general(low, ret[...], over, preferred_element_type=f32)
    ).astype(bf16)

    sent = [kv_pass(col)] + list(disp.values())
    sent += [relay(d, dy) for d in range(1, n_ep) for dy in range(1, ny)]
    sent += [cross(c, dy) for c in range(2) for dy in range(ny)]
    sent += [m1(c) for c in range(2)]
    sent += [m2(c, s, dy) for c in range(2) for s in range(2) for dy in range(1, ny)]
    sent += [back(d) for d in range(1, n_ep)]
    sent += [a1(d) for d in range(ny)] + [a2(d) for d in range(1, ny)]
    for copy in sent:
        copy.wait_send()

    @pl.when(has_next)
    def _():
        kv_line(col, col + 1, col).wait_send()

    @pl.when(has_prev)
    def _():
        kv_line(col, col - 1, nz).wait_send()

    def kv_done(k, carry):
        b, target = line_step(k)

        @pl.when(jnp.logical_and(target >= 0, target <= nz - 1))
        def _():
            kv_line(b, target, b).wait_send()

        kv_pass(b).wait_send()
        return carry

    lax.fori_loop(0, nz - 1, kv_done, 0)


def per_device(
    n_ep, n_tp,
    q_in, k_in, v_in, q_gain, k_gain, w_out, post_gain,
    moe_in, routes, route_logits, pre_gain, w_gate, w_up, w_down,
):
    bf16 = jnp.bfloat16
    head = q_gain.shape[0]
    rows = q_in.shape[0]
    heads = q_in.shape[1] // head
    kv_count = k_in.shape[1] // head
    repeat = heads * n_tp // kv_count
    ny = n_tp // 2
    nz = n_ep // 2
    grid_rows = turn_tables(n_ep * rows, GRID_W, head // 4)

    tokens, top = routes.shape
    width = moe_in.shape[1]
    dq = width // n_tp
    need = max(2, 3 * top * tokens // (2 * n_ep))
    cap = -(-need // 16) * 16
    slots = n_ep * cap

    piece = rows // n_tp
    ff = w_gate.shape[2]
    dma = pltpu.SemaphoreType.DMA
    vmem = pl.BlockSpec(memory_space=pltpu.VMEM)
    hbm = pl.BlockSpec(memory_space=pl.ANY)
    return pl.pallas_call(
        functools.partial(kernel, (n_ep, n_tp, heads, cap, repeat)),
        out_shape=(
            jax.ShapeDtypeStruct((piece, width), bf16),
            jax.ShapeDtypeStruct((tokens, dq), bf16),
        ),
        in_specs=[vmem] * 10 + [hbm] * 8,
        out_specs=(vmem, vmem),
        scratch_shapes=[
            pltpu.VMEM((rows, heads * head), bf16),
            pltpu.VMEM((rows, 2 * head), bf16),
            pltpu.VMEM((rows, 2 * head), bf16),
            pltpu.VMEM((tokens, width), bf16),
            pltpu.VMEM((heads * head, width), bf16),
            pltpu.VMEM((heads * rows, 2 * head), bf16),
            pltpu.VMEM((slots, tokens), bf16),
            pltpu.VMEM((slots, dq), bf16),
            pltpu.VMEM((slots, tokens), jnp.float32),
            pltpu.VMEM((width, ff), bf16),
            pltpu.VMEM((width, ff), bf16),
            pltpu.VMEM((ff, width), bf16),
            pltpu.VMEM((n_ep, rows, 2 * head), bf16),
            pltpu.VMEM((2, rows, 2 * head), bf16),
            pltpu.VMEM((2, 2 * head, rows), bf16),
            pltpu.VMEM((heads * rows, 2 * head), jnp.float32),
            pltpu.VMEM((slots, width), bf16),
            pltpu.VMEM((slots, ff), bf16),
            pltpu.VMEM((ny, piece, width), bf16),
            pltpu.VMEM((ny, piece, width), bf16),
            pltpu.VMEM((ny, piece, width), bf16),
            pltpu.VMEM((ny, piece, width), bf16),
            pltpu.VMEM((2, 2, ny, slots // 2, dq), bf16),
            pltpu.VMEM((2, ny, slots // 2, dq), bf16),
            pltpu.VMEM((2, ny, slots // 2, dq), bf16),
            pltpu.VMEM((2, ny, slots // 2, dq), bf16),
            pltpu.VMEM((slots, dq), bf16),
            pltpu.VMEM((slots, dq), bf16),
            dma((5,)), dma((3,)),
            dma((nz + 1,)), dma((nz,)), dma((nz,)), dma((nz,)),
            dma((n_ep,)), dma((n_ep,)), dma((n_ep, ny)), dma((n_ep, ny)),
            dma((2,)), dma((2,)), dma((2, ny)), dma((2, ny)),
            dma((ny,)), dma((ny,)), dma((ny,)), dma((ny,)),
            dma((2,)), dma((2,)), dma((2, 2, ny)), dma((2, 2, ny)),
            dma((n_ep,)), dma((n_ep,)),
        ],
        compiler_params=pltpu.CompilerParams(
            collective_id=0, has_side_effects=True, vmem_limit_bytes=60 * 1024 * 1024
        ),
    )(
        routes.T, route_logits.T, pre_gain[None, :], post_gain[None, :], q_gain[None, :], k_gain[None, :], *grid_rows,
        q_in, k_in, v_in, moe_in, w_out, w_gate[0], w_up[0], w_down[0],
    )


def solution(mesh):
    return jax.shard_map(
        functools.partial(per_device, mesh.shape["ep"], mesh.shape["tp"]),
        mesh=mesh,
        in_specs=(
            P("ep", "tp"),
            P("ep", None),
            P("ep", None),
            P(),
            P(),
            P("tp", None),
            P(),
            P("ep", None),
            P("ep", None),
            P("ep", None),
            P(),
            P("ep", None, "tp"),
            P("ep", None, "tp"),
            P("ep", "tp", None),
        ),
        out_specs=(P(("ep", "tp"), None), P("ep", "tp")),
        check_vma=False,
    )
```

time: 77.2 us -> 65 us (0.84)
  the two profiles are of different devices: /device:TPU:0 before, /device:TPU:25 now
where the time goes in v2:
time: 65 us; the launch traced here: 64.8 us
  Pallas kernels  60.7 us (93%)
  local copies, waits for them, and re-layouts  3.45 us (5%)
    pallas_call x1, Pallas kernels, per_device(): pl.pallas_call(functools.partial(kernel, (n_ep, n_tp, heads, cap, repeat)...  60.7 us
    unnamed x2, local copies, waits for them, and re-layouts  3.45 us

profile of v2, /device:TPU:25, one launch (start us, length us, event | category | flops | bytes accessed | tf_op | source)
XLA Modules:
  0.0 64.8 jit_solution(11855862439888646179)
XLA Ops:
  0.6 60.7 %shard_map.185 = (bf16[128,2048]{1,0:T(8,128)(2,1)}, bf16[128,512]{1,0:T(8,128)(2,1)}) custom-call(s32[2,128]{1,0:T(2,128)} %bitcast.14, f32[2,128]{1,0:T(2,128)} %bitcast.15, f32[1,2048]{1,0:T(1,128)} %bitcast.12, f32[1,2048]{1,0:T(1,128)} %bitcast.13, f32[1,64]{1,0:T(1,128)} %bitcast.16, f32[1,64]{1,0:T(1,128)} %bitcast.17, ...), custom_call_target="tpu_custom_call" | custom-call | tf_op jit(solution)/shard_map/pallas_call | solution.py:586
  61.3 1.9 %copy.22 = bf16[128,2048]{1,0:T(8,128)(2,1)} copy(bf16[128,2048]{1,0:T(8,128)(2,1)} %get-tuple-element.4) | data formatting | bytes 1048576
  63.2 1.6 %copy.23 = bf16[128,512]{1,0:T(8,128)(2,1)} copy(bf16[128,512]{1,0:T(8,128)(2,1)} %get-tuple-element.5) | data formatting | bytes 262144

commit v3 on v2

--- a/solution.py
+++ b/solution.py
@@ -12,6 +12,8 @@
 EPSILON = 1e-06
 ROPE_BASE = 10000.0
 MESH = pl.DeviceIdType.MESH
+SKEW = 128
+VMEM_LIMIT = 60 * 1024 * 1024
 
 
 def turn_tables(positions, rows_of_grid, quarter):
@@ -29,14 +31,15 @@
     grid_rows = positions // rows_of_grid
     by_row = table(grid_rows, True)
     by_col = table(rows_of_grid, False)
-    return [jnp.asarray(part, jnp.float32) for part in by_row + by_col]
+    return jnp.asarray(np.concatenate(by_row + by_col), jnp.float32)
 
 
 def kernel(
     dims,
-    route_ref, logit_ref, pre_ref, gain_ref, qg_ref, kg_ref, crow_ref, srow_ref, ccol_ref, scol_ref,
+    route_hbm, logit_hbm, pre_hbm, gain_hbm, qg_hbm, kg_hbm, turn_hbm,
     q_hbm, k_hbm, v_hbm, x_hbm, wout_hbm, wg_hbm, wu_hbm, wd_hbm,
     attn_ref, moe_ref,
+    route_ref, logit_ref, pre_ref, gain_ref, qg_ref, kg_ref, turn_ref,
     q_in, k_in, v_in, x_ref, wout_ref, q_ref, placed_ref,
     outgo_ref, mixw_ref, wg, wu, wd, kvbuf, vx, kt, acc, arrived, hidden,
     pa, pa_in, pa_red, pa_in2, pm, pm_in, pm_red, pm_in2, summed, ret,
@@ -89,6 +92,9 @@
     def slot_rows(e):
         return pl.ds(pl.multiple_of(e * cap, cap), cap)
 
+    def cols_of(ref):
+        return pl.ds(0, ref.shape[1])
+
     def lanes_of(t):
         return pl.ds(pl.multiple_of(t * dq, dq), dq)
 
@@ -105,23 +111,26 @@
     def held(d):
         return pl.ds(order.index(d) * cap, cap)
 
-    head = qg_ref.shape[1]
+    head = qg_hbm.shape[1]
     lane_count = 2 * head
     kv_index = lax.div(tp * heads, repeat)
     kv_lanes = pl.ds(pl.multiple_of(lax.div(kv_index, 2) * lane_count, lane_count), lane_count)
     ins = [
         pltpu.make_async_copy(src, dst, in_sem.at[i])
         for i, (src, dst) in enumerate((
-            (x_hbm, x_ref), (k_hbm.at[:, kv_lanes], k_in), (v_hbm.at[:, kv_lanes], v_in),
-            (q_hbm, q_in), (wout_hbm, wout_ref),
+            (route_hbm, route_ref), (logit_hbm, logit_ref), (x_hbm, x_ref), (pre_hbm, pre_ref),
+            (k_hbm.at[:, kv_lanes], k_in), (v_hbm.at[:, kv_lanes], v_in), (turn_hbm, turn_ref), (kg_hbm, kg_ref),
+            (q_hbm, q_in), (qg_hbm, qg_ref), (gain_hbm, gain_ref), (wout_hbm, wout_ref.at[:, cols_of(wout_hbm)]),
         ))
     ]
-    for copy in ins[:4]:
+    for copy in ins:
         copy.start()
     loads = [
         pltpu.make_async_copy(src, dst, w_sem.at[i])
-        for i, (src, dst) in enumerate(((wg_hbm, wg), (wu_hbm, wu), (wd_hbm, wd)))
+        for i, (src, dst) in enumerate(((wg_hbm, wg.at[:, cols_of(wg_hbm)]), (wu_hbm, wu.at[:, cols_of(wu_hbm)]), (wd_hbm, wd.at[:, cols_of(wd_hbm)])))
     ]
+    for copy in loads:
+        copy.start()
     barrier = pltpu.get_barrier_semaphore()
     for d in range(1, n_ep):
         pl.semaphore_signal(barrier, inc=1, device_id=(ep_at(d), tp), device_id_type=MESH)
@@ -130,6 +139,8 @@
     pl.semaphore_signal(barrier, inc=1, device_id=(ep, partner), device_id_type=MESH)
 
     top, tokens = logit_ref.shape
+    ins[0].wait()
+    ins[1].wait()
     logits = logit_ref[...]
     power = jnp.exp(logits - jnp.max(logits, axis=0, keepdims=True))
     chance = power / jnp.sum(power, axis=0, keepdims=True)
@@ -151,7 +162,8 @@
         placed_ref[e * cap : (e + 1) * cap, :] = jnp.where(there, 1.0, 0.0).astype(bf16)
         mixw_ref[e * cap : (e + 1) * cap, :] = jnp.where(there, share[e : e + 1, :], 0.0)
 
-    ins[0].wait()
+    ins[2].wait()
+    ins[3].wait()
     x = x_ref[...].astype(f32)
     scale = lax.rsqrt(jnp.mean(x * x, axis=-1, keepdims=True) + EPSILON)
     mine = pl.ds(pl.multiple_of(tp * dq, dq), dq)
@@ -180,14 +192,15 @@
             pltpu.roll(values, lane_count - head // 4, 1),
             pltpu.roll(values, head // 4, 1),
         )
-        at = pl.ds(ep * blocks + b, 1)
-        return values * (crow_ref[at, :] + ccol_ref[...]) + other * (srow_ref[at, :] + scol_ref[...])
-
+        lines = turn_ref.shape[0] // 2 - GRID_W
+        cos = turn_ref[pl.ds(ep * blocks + b, 1), :] + turn_ref[2 * lines : 2 * lines + GRID_W, :]
+        sin = turn_ref[pl.ds(lines + ep * blocks + b, 1), :] + turn_ref[2 * lines + GRID_W :, :]
+        return values * cos + other * sin
+
+    odd = lax.rem(kv_index, 2)
+    for copy in ins[4:8]:
+        copy.wait()
     k_gain = jnp.concatenate([kg_ref[...], kg_ref[...]], axis=1)
-    q_gain = jnp.concatenate([qg_ref[...], qg_ref[...]], axis=1)
-    odd = lax.rem(kv_index, 2)
-    ins[1].wait()
-    ins[2].wait()
     for b in range(blocks):
         at = slice(b * GRID_W, (b + 1) * GRID_W)
         keys = turned(k_in[at, :].astype(f32), k_gain, b)
@@ -230,11 +243,9 @@
 
     for d in groups[1]:
         disp[d].start()
-    for copy in loads:
-        copy.start()
-    ins[4].start()
-
-    ins[3].wait()
+    ins[8].wait()
+    ins[9].wait()
+    q_gain = jnp.concatenate([qg_ref[...], qg_ref[...]], axis=1)
     for g in range(max(1, heads // 2)):
         for b in range(blocks):
             at = slice(b * GRID_W, (b + 1) * GRID_W)
@@ -282,11 +293,8 @@
     def attend(e, fresh):
         prepare(e, 0)
 
-        def one(i, carry):
+        for i in range(q_rows // (2 * tile)):
             attend_rows(i, 0, fresh)
-            return carry
-
-        lax.fori_loop(0, q_rows // (2 * tile), one, 0)
 
     shorter = jnp.minimum(col, nz - 1 - col)
     longer = jnp.where(col <= nz - 1 - col, 1, -1)
@@ -318,6 +326,13 @@
         @pl.when(jnp.logical_and(opening, both))
         def _():
             line_one(k + 1)
+
+    def line_end(early):
+        middle = shorter > 0
+
+        @pl.when(middle if early else jnp.logical_not(middle))
+        def _():
+            line_one(nz - 1 - 1)
 
     def line_block(k):
         return line_step(k)[0] * 2 + side
@@ -362,8 +377,8 @@
                     wait("relay", relay(d, dy))
             cross(c, dy).start()
 
-    ff = hidden.shape[1]
-    step = min(256, ff)
+    ff = wg_hbm.shape[1]
+    step = min(512, ff)
 
     def m1(c):
         return remote(pm.at[c, 1 - core], pm_in.at[c], m1_s.at[c], m1_r.at[c], ep, partner)
@@ -373,35 +388,38 @@
         return remote(pm_red.at[c, lax.rem(row + dy, ny), at], pm_in2.at[c, row, at],
                       m2_s.at[c, s, dy], m2_r.at[c, s, dy], ep, same_core(dy))
 
-    def experts(c):
+    def chunk_rows(c):
+        return slice(c * chunk, (c + 1) * chunk)
+
+    def experts_up(c):
         for dy in range(ny):
             wait("cross", cross(c, dy))
         if c == 0:
             loads[0].wait()
             loads[1].wait()
-        rows = slice(c * chunk, (c + 1) * chunk)
+        rows = chunk_rows(c)
 
         def gated(i, carry):
             at = pl.ds(pl.multiple_of(i * step, step), step)
-            x = arrived[rows, :]
+            x = arrived[rows, : wg_hbm.shape[0]]
             gate = jnp.dot(x, wg[:, at], preferred_element_type=f32)
             up = jnp.dot(x, wu[:, at], preferred_element_type=f32)
             hidden[rows, at] = (gate / (1.0 + jnp.exp(-gate)) * up).astype(bf16)
             return carry
 
         lax.fori_loop(0, ff // step, gated, 0)
+
+    def experts_down(c):
+        rows = chunk_rows(c)
         if c == 0:
             loads[2].wait()
 
         def down_for(which):
-            def down(y, carry):
+            for y in range(ny):
                 cols = pl.ds(pl.multiple_of((y * 2 + which) * dq, dq), dq)
                 pm[c, which, y] = jnp.dot(
-                    hidden[rows, :], wd[:, cols], preferred_element_type=f32
+                    hidden[rows, :ff], wd[:, cols], preferred_element_type=f32
                 ).astype(bf16)
-                return carry
-
-            lax.fori_loop(0, ny, down, 0)
 
         down_for(1 - core)
         m1(c).start()
@@ -453,13 +471,14 @@
                 pieces.append((sums[:, half:] / sums[:, :half]).astype(bf16))
             sides.append(pieces[0] if heads == 1 else jnp.concatenate(pieces, axis=1))
         both = jnp.concatenate(sides, axis=0)
-        return jnp.dot(both, wout_ref[...], preferred_element_type=f32)
+        return jnp.dot(both, wout_ref[:, : wout_hbm.shape[1]], preferred_element_type=f32)
 
     def a1(d):
         return remote(pa.at[d], pa_in.at[d], a1_s.at[d], a1_r.at[d], ep, partner)
 
-    def a2(d):
-        return remote(pa_red.at[d], pa_in2.at[d], a2_s.at[d], a2_r.at[d], ep, same_core(d))
+    def a2(d, s):
+        at = pl.ds(s * (piece // 2), piece // 2)
+        return remote(pa_red.at[d, at], pa_in2.at[d, at], a2_s.at[d, s], a2_r.at[d, s], ep, same_core(d))
 
     def finish_start(d):
         total = finish(lax.rem(row + d, ny)).astype(bf16)
@@ -476,44 +495,50 @@
     attend(mate, False)
     relay_chunk(0)
     split = max(1, (nz - 1) // 2)
+    brief = nz - 2 == split + 1
     line_take(0)
     attend(line_block(0), False)
     relay_chunk(1)
+    cross_chunk(0)
     attend(pass_block(0), False)
     lax.fori_loop(1, split, take, 0)
-    cross_chunk(0)
+    if brief:
+        line_end(True)
+    with jax.named_scope("up0"):
+        experts_up(0)
     line_take(split)
+    with jax.named_scope("down0"):
+        experts_down(0)
     attend(line_block(split), False)
-    with jax.named_scope("experts0"):
-        experts(0)
+    reduce_cores(0)
+    if brief:
+        line_end(False)
     cross_chunk(1)
     attend(pass_block(split), False)
-    reduce_cores(0)
     lax.fori_loop(split + 1, nz - 2, take, 0)
-    line_take(nz - 2)
+    if not brief:
+        line_take(nz - 2)
     prepare(line_block(nz - 2), 0)
-    with jax.named_scope("experts1"):
-        experts(1)
+    with jax.named_scope("up1"):
+        experts_up(1)
+    with jax.named_scope("down1"):
+        experts_down(1)
+    prepare(pass_block(nz - 2), 1)
+    ins[10].wait()
+    ins[11].wait()
+    for d in range(1, ny):
+        with jax.named_scope("finish"):
+            finish_start(d)
+    reduce_cores(1)
     send_back(0)
-    prepare(pass_block(nz - 2), 1)
-    ins[4].wait()
-    reduce_cores(1)
-    for d in range(1, ny):
-        with jax.named_scope("finish_other"):
-            finish_start(d)
     for d in range(1, ny):
         pa_red[d] = finish_end(d).astype(bf16)
-        a2(d).start()
+        for s in range(2):
+            a2(d, s).start()
+    with jax.named_scope("finish"):
+        finish_start(0)
     send_back(1)
-    with jax.named_scope("finish_own"):
-        finish_start(0)
-    mixed = finish_end(0).astype(bf16).astype(f32)
-    for d in range(1, ny):
-        wait("a2", a2(d))
-        mixed = mixed + pa_in2[d].astype(f32)
-    square = jnp.mean(mixed * mixed, axis=-1, keepdims=True)
-    attn_ref[...] = (mixed * lax.rsqrt(square + EPSILON) * gain_ref[...]).astype(bf16)
-
+    pa_red[0] = finish_end(0).astype(bf16)
     for d in range(1, n_ep):
         wait("back", back(d))
     mixw = mixw_ref[...]
@@ -524,6 +549,14 @@
         lax.dot_general(high, ret[...], over, preferred_element_type=f32)
         + lax.dot_general(low, ret[...], over, preferred_element_type=f32)
     ).astype(bf16)
+    for s in range(2):
+        at = slice(s * (piece // 2), (s + 1) * (piece // 2))
+        mixed = pa_red[0, at].astype(f32)
+        for d in range(1, ny):
+            wait("a2", a2(d, s))
+            mixed = mixed + pa_in2[d, at].astype(f32)
+        square = jnp.mean(mixed * mixed, axis=-1, keepdims=True)
+        attn_ref[at, :] = (mixed * lax.rsqrt(square + EPSILON) * gain_ref[...]).astype(bf16)
 
     sent = [kv_pass(col)] + list(disp.values())
     sent += [relay(d, dy) for d in range(1, n_ep) for dy in range(1, ny)]
@@ -531,7 +564,7 @@
     sent += [m1(c) for c in range(2)]
     sent += [m2(c, s, dy) for c in range(2) for s in range(2) for dy in range(1, ny)]
     sent += [back(d) for d in range(1, n_ep)]
-    sent += [a1(d) for d in range(ny)] + [a2(d) for d in range(1, ny)]
+    sent += [a1(d) for d in range(ny)] + [a2(d, s) for d in range(1, ny) for s in range(2)]
     for copy in sent:
         copy.wait_send()
 
@@ -569,7 +602,7 @@
     repeat = heads * n_tp // kv_count
     ny = n_tp // 2
     nz = n_ep // 2
-    grid_rows = turn_tables(n_ep * rows, GRID_W, head // 4)
+    turns = turn_tables(n_ep * rows, GRID_W, head // 4)
 
     tokens, top = routes.shape
     width = moe_in.shape[1]
@@ -586,30 +619,37 @@
     return pl.pallas_call(
         functools.partial(kernel, (n_ep, n_tp, heads, cap, repeat)),
         out_shape=(
-            jax.ShapeDtypeStruct((piece, width), bf16),
-            jax.ShapeDtypeStruct((tokens, dq), bf16),
+            pltpu.VMEM((piece, width), bf16),
+            pltpu.VMEM((tokens, dq), bf16),
         ),
-        in_specs=[vmem] * 10 + [hbm] * 8,
+        in_specs=[hbm] * 15,
         out_specs=(vmem, vmem),
         scratch_shapes=[
+            pltpu.VMEM((top, tokens), jnp.int32),
+            pltpu.VMEM((top, tokens), jnp.float32),
+            pltpu.VMEM((1, width), jnp.float32),
+            pltpu.VMEM((1, width), jnp.float32),
+            pltpu.VMEM((1, head), jnp.float32),
+            pltpu.VMEM((1, head), jnp.float32),
+            pltpu.VMEM(turns.shape, jnp.float32),
             pltpu.VMEM((rows, heads * head), bf16),
             pltpu.VMEM((rows, 2 * head), bf16),
             pltpu.VMEM((rows, 2 * head), bf16),
             pltpu.VMEM((tokens, width), bf16),
-            pltpu.VMEM((heads * head, width), bf16),
+            pltpu.VMEM((heads * head, width + SKEW), bf16),
             pltpu.VMEM((heads * rows, 2 * head), bf16),
             pltpu.VMEM((slots, tokens), bf16),
             pltpu.VMEM((slots, dq), bf16),
             pltpu.VMEM((slots, tokens), jnp.float32),
-            pltpu.VMEM((width, ff), bf16),
-            pltpu.VMEM((width, ff), bf16),
-            pltpu.VMEM((ff, width), bf16),
+            pltpu.VMEM((width, ff + SKEW), bf16),
+            pltpu.VMEM((width, ff + SKEW), bf16),
+            pltpu.VMEM((ff, width + SKEW), bf16),
             pltpu.VMEM((n_ep, rows, 2 * head), bf16),
             pltpu.VMEM((2, rows, 2 * head), bf16),
             pltpu.VMEM((2, 2 * head, rows), bf16),
             pltpu.VMEM((heads * rows, 2 * head), jnp.float32),
-            pltpu.VMEM((slots, width), bf16),
-            pltpu.VMEM((slots, ff), bf16),
+            pltpu.VMEM((slots, width + SKEW), bf16),
+            pltpu.VMEM((slots, ff + SKEW), bf16),
             pltpu.VMEM((ny, piece, width), bf16),
             pltpu.VMEM((ny, piece, width), bf16),
             pltpu.VMEM((ny, piece, width), bf16),
@@ -620,19 +660,19 @@
             pltpu.VMEM((2, ny, slots // 2, dq), bf16),
             pltpu.VMEM((slots, dq), bf16),
             pltpu.VMEM((slots, dq), bf16),
-            dma((5,)), dma((3,)),
+            dma((12,)), dma((3,)),
             dma((nz + 1,)), dma((nz,)), dma((nz,)), dma((nz,)),
             dma((n_ep,)), dma((n_ep,)), dma((n_ep, ny)), dma((n_ep, ny)),
             dma((2,)), dma((2,)), dma((2, ny)), dma((2, ny)),
-            dma((ny,)), dma((ny,)), dma((ny,)), dma((ny,)),
+            dma((ny,)), dma((ny,)), dma((ny, 2)), dma((ny, 2)),
             dma((2,)), dma((2,)), dma((2, 2, ny)), dma((2, 2, ny)),
             dma((n_ep,)), dma((n_ep,)),
         ],
         compiler_params=pltpu.CompilerParams(
-            collective_id=0, has_side_effects=True, vmem_limit_bytes=60 * 1024 * 1024
+            collective_id=0, has_side_effects=True, vmem_limit_bytes=VMEM_LIMIT
         ),
     )(
-        routes.T, route_logits.T, pre_gain[None, :], post_gain[None, :], q_gain[None, :], k_gain[None, :], *grid_rows,
+        routes.T, route_logits.T, pre_gain[None, :], post_gain[None, :], q_gain[None, :], k_gain[None, :], turns,
         q_in, k_in, v_in, moe_in, w_out, w_gate[0], w_up[0], w_down[0],
     )
 

time: 65 us -> 53.8 us (0.83)
  the two profiles are of different devices: /device:TPU:25 before, /device:TPU:0 now
where the time goes in v3:
time: 53.8 us; the launch traced here: 53.4 us
  Pallas kernels  51.3 us (95%)
  local copies, waits for them, and re-layouts  1.45 us (3%)
  between operations  0.64 us (1%)
    pallas_call x1, Pallas kernels, per_device(): pl.pallas_call(functools.partial(kernel, (n_ep, n_tp, heads, cap, repeat)...  51.3 us
    unnamed x2, local copies, waits for them, and re-layouts  1.45 us

profile of v3, /device:TPU:0, one launch (start us, length us, event | category | flops | bytes accessed | tf_op | source)
XLA Modules:
  0.0 53.4 jit_solution(8374486985492766618)
XLA Ops:
  0.6 51.3 %shard_map.158 = (bf16[128,2048]{1,0:T(8,128)(2,1)S(1)}, bf16[128,512]{1,0:T(8,128)(2,1)S(1)}) custom-call(s32[2,128]{1,0:T(2,128)} %bitcast.14, f32[2,128]{1,0:T(2,128)} %bitcast.15, f32[1,2048]{1,0:T(1,128)} %bitcast.12, f32[1,2048]{1,0:T(1,128)} %bitcast.13, f32[1,64]{1,0:T(1,128)} %bitcast.16, f32[1,64]{1,0:T(1,128)} %bitcast.17, ...), custom_call_target="tpu_custom_call" | custom-call | tf_op jit(solution)/shard_map/pallas_call | solution.py:619
  52.0 0.8 %copy.19 = bf16[128,2048]{1,0:T(8,128)(2,1)} copy(bf16[128,2048]{1,0:T(8,128)(2,1)S(1)} %get-tuple-element.2) | data formatting | bytes 1048576
  52.8 0.7 %copy.20 = bf16[128,512]{1,0:T(8,128)(2,1)} copy(bf16[128,512]{1,0:T(8,128)(2,1)S(1)} %get-tuple-element.3) | data formatting | bytes 262144

commit v4 on v3

--- a/solution.py
+++ b/solution.py
@@ -42,9 +42,9 @@
     route_ref, logit_ref, pre_ref, gain_ref, qg_ref, kg_ref, turn_ref,
     q_in, k_in, v_in, x_ref, wout_ref, q_ref, placed_ref,
     outgo_ref, mixw_ref, wg, wu, wd, kvbuf, vx, kt, acc, arrived, hidden,
-    pa, pa_in, pa_red, pa_in2, pm, pm_in, pm_red, pm_in2, summed, ret,
+    wall, ho_out, ho_in, whole, pa, pa_in, pa_red, pa_in2, pm, pm_in, pm_red, pm_in2, summed, ret,
     in_sem, w_sem, kz_s, kz_r, kx_s, kx_r, disp_s, disp_r, rel_s, rel_r, c0_s, c0_r, cy_s, cy_r,
-    a1_s, a1_r, a2_s, a2_r, m1_s, m1_r, m2_s, m2_r, ret_s, ret_r,
+    w0_s, w0_r, wy_s, wy_r, wc_s, wc_r, ho_s, ho_r, a1_s, a1_r, a2_s, a2_r, m1_s, m1_r, m2_s, m2_r, ret_s, ret_r,
 ):
     n_ep, n_tp, heads, cap, repeat = dims
     ny = n_tp // 2
@@ -95,6 +95,33 @@
     def cols_of(ref):
         return pl.ds(0, ref.shape[1])
 
+    narrow = pa.shape[2]
+    wide = wout_hbm.shape[1] - narrow
+    dims_here = wout_hbm.shape[0]
+    parts = wy_s.shape[1]
+    strip = dims_here // parts
+    starts = (parts * 5 // 8, parts * 7 // 8)
+
+    def wall_rows(t, i, count):
+        first_row = pl.multiple_of(t * dims_here + i * strip, strip)
+        return wall.at[pl.ds(first_row, count * strip), pl.ds(0, wide)]
+
+    def w_partner():
+        block = wall_rows(tp, 0, parts)
+        return remote(block, block, w0_s.at[0], w0_r.at[0], ep, partner)
+
+    def w_row(dy, i):
+        block = wall_rows(tp, i, 1)
+        return remote(block, block, wy_s.at[dy, i], wy_r.at[dy, i], ep, same_core(dy))
+
+    def w_cross(dy):
+        block = wall_rows(row_from(dy) * 2 + core, 0, parts)
+        return remote(block, block, wc_s.at[dy], wc_r.at[dy], ep, partner)
+
+    def w_send(i):
+        for dy in range(1, ny):
+            w_row(dy, i).start()
+
     def lanes_of(t):
         return pl.ds(pl.multiple_of(t * dq, dq), dq)
 
@@ -120,7 +147,8 @@
         for i, (src, dst) in enumerate((
             (route_hbm, route_ref), (logit_hbm, logit_ref), (x_hbm, x_ref), (pre_hbm, pre_ref),
             (k_hbm.at[:, kv_lanes], k_in), (v_hbm.at[:, kv_lanes], v_in), (turn_hbm, turn_ref), (kg_hbm, kg_ref),
-            (q_hbm, q_in), (qg_hbm, qg_ref), (gain_hbm, gain_ref), (wout_hbm, wout_ref.at[:, cols_of(wout_hbm)]),
+            (q_hbm, q_in), (qg_hbm, qg_ref), (gain_hbm, gain_ref), (wout_hbm.at[:, pl.ds(0, narrow)], wout_ref.at[:, pl.ds(0, narrow)]),
+            (wout_hbm.at[:, pl.ds(narrow, wide)], wall_rows(tp, 0, parts)),
         ))
     ]
     for copy in ins:
@@ -228,10 +256,10 @@
     has_next = col < nz - 1
     has_prev = col > 0
 
-    kv_pass(col).start()
     for d in groups[0]:
         if d:
             disp[d].start()
+    kv_pass(col).start()
 
     @pl.when(has_next)
     def _():
@@ -243,6 +271,10 @@
 
     for d in groups[1]:
         disp[d].start()
+    ins[12].wait()
+    for i in range(starts[0]):
+        w_send(i)
+    w_partner().start()
     ins[8].wait()
     ins[9].wait()
     q_gain = jnp.concatenate([qg_ref[...], qg_ref[...]], axis=1)
@@ -470,8 +502,7 @@
                 sums = acc[at, :]
                 pieces.append((sums[:, half:] / sums[:, :half]).astype(bf16))
             sides.append(pieces[0] if heads == 1 else jnp.concatenate(pieces, axis=1))
-        both = jnp.concatenate(sides, axis=0)
-        return jnp.dot(both, wout_ref[:, : wout_hbm.shape[1]], preferred_element_type=f32)
+        return sides
 
     def a1(d):
         return remote(pa.at[d], pa_in.at[d], a1_s.at[d], a1_r.at[d], ep, partner)
@@ -480,8 +511,20 @@
         at = pl.ds(s * (piece // 2), piece // 2)
         return remote(pa_red.at[d, at], pa_in2.at[d, at], a2_s.at[d, s], a2_r.at[d, s], ep, same_core(d))
 
+    def ho(d, c):
+        target = lax.rem(row + d, ny) * 2 + (core if c else 1 - core)
+        return remote(ho_out.at[2 * d + c], ho_in.at[tp], ho_s.at[2 * d + c], ho_r.at[2 * d + c], ep, target)
+
     def finish_start(d):
-        total = finish(lax.rem(row + d, ny)).astype(bf16)
+        sides = finish(lax.rem(row + d, ny))
+        for c in range(2):
+            if d == 0 and c == 1:
+                ho_in[tp] = sides[1]
+            else:
+                ho_out[2 * d + c] = sides[c]
+                ho(d, c).start()
+        both = jnp.concatenate(sides, axis=0)
+        total = jnp.dot(both, wout_ref[:, :narrow], preferred_element_type=f32).astype(bf16)
         pa[d] = total[:piece]
         a1(d).start()
         pa_red[d] = total[piece:]
@@ -491,14 +534,16 @@
         return pa_red[d].astype(f32) + pa_in[d].astype(f32)
 
     attend(ep, True)
+    relay_chunk(0)
     wait("kv_mate", kv_pass(col))
     attend(mate, False)
-    relay_chunk(0)
     split = max(1, (nz - 1) // 2)
     brief = nz - 2 == split + 1
     line_take(0)
     attend(line_block(0), False)
     relay_chunk(1)
+    for i in range(*starts):
+        w_send(i)
     cross_chunk(0)
     attend(pass_block(0), False)
     lax.fori_loop(1, split, take, 0)
@@ -509,28 +554,34 @@
     line_take(split)
     with jax.named_scope("down0"):
         experts_down(0)
+    cross_chunk(1)
     attend(line_block(split), False)
     reduce_cores(0)
+    for i in range(starts[1], parts):
+        w_send(i)
+    with jax.named_scope("up1"):
+        experts_up(1)
     if brief:
         line_end(False)
-    cross_chunk(1)
+    with jax.named_scope("down1"):
+        experts_down(1)
     attend(pass_block(split), False)
     lax.fori_loop(split + 1, nz - 2, take, 0)
     if not brief:
         line_take(nz - 2)
+    reduce_cores(1)
+    send_back(0)
     prepare(line_block(nz - 2), 0)
-    with jax.named_scope("up1"):
-        experts_up(1)
-    with jax.named_scope("down1"):
-        experts_down(1)
     prepare(pass_block(nz - 2), 1)
     ins[10].wait()
     ins[11].wait()
     for d in range(1, ny):
         with jax.named_scope("finish"):
             finish_start(d)
-    reduce_cores(1)
-    send_back(0)
+    for dy in range(1, ny):
+        for i in range(parts):
+            wait("w_row", w_row(dy, i))
+        w_cross(dy).start()
     for d in range(1, ny):
         pa_red[d] = finish_end(d).astype(bf16)
         for s in range(2):
@@ -539,6 +590,27 @@
         finish_start(0)
     send_back(1)
     pa_red[0] = finish_end(0).astype(bf16)
+    wait("w_partner", w_partner())
+    for dy in range(1, ny):
+        wait("w_cross", w_cross(dy))
+    for d in range(ny):
+        for c in range(2):
+            if d or c == 0:
+                wait("ho", ho(d, c))
+    gathered = jnp.concatenate([ho_in[t] for t in range(n_tp)], axis=1)
+    whole[...] = jnp.dot(gathered, wall[:, :wide], preferred_element_type=f32)
+    for s in range(2):
+        at = slice(s * (piece // 2), (s + 1) * (piece // 2))
+        mixed = pa_red[0, at].astype(f32)
+        for d in range(1, ny):
+            wait("a2", a2(d, s))
+            mixed = mixed + pa_in2[d, at].astype(f32)
+        rest = whole[at, :]
+        square = jnp.sum(mixed * mixed, axis=-1, keepdims=True) + jnp.sum(rest * rest, axis=-1, keepdims=True)
+        scale = lax.rsqrt(square * (1.0 / (narrow + wide)) + EPSILON)
+        attn_ref[at, :narrow] = (mixed * scale * gain_ref[:, :narrow]).astype(bf16)
+        attn_ref[at, narrow:] = (rest * scale * gain_ref[:, narrow:]).astype(bf16)
+
     for d in range(1, n_ep):
         wait("back", back(d))
     mixw = mixw_ref[...]
@@ -549,21 +621,15 @@
         lax.dot_general(high, ret[...], over, preferred_element_type=f32)
         + lax.dot_general(low, ret[...], over, preferred_element_type=f32)
     ).astype(bf16)
-    for s in range(2):
-        at = slice(s * (piece // 2), (s + 1) * (piece // 2))
-        mixed = pa_red[0, at].astype(f32)
-        for d in range(1, ny):
-            wait("a2", a2(d, s))
-            mixed = mixed + pa_in2[d, at].astype(f32)
-        square = jnp.mean(mixed * mixed, axis=-1, keepdims=True)
-        attn_ref[at, :] = (mixed * lax.rsqrt(square + EPSILON) * gain_ref[...]).astype(bf16)
-
     sent = [kv_pass(col)] + list(disp.values())
     sent += [relay(d, dy) for d in range(1, n_ep) for dy in range(1, ny)]
     sent += [cross(c, dy) for c in range(2) for dy in range(ny)]
     sent += [m1(c) for c in range(2)]
     sent += [m2(c, s, dy) for c in range(2) for s in range(2) for dy in range(1, ny)]
     sent += [back(d) for d in range(1, n_ep)]
+    sent += [w_partner()] + [w_row(dy, i) for dy in range(1, ny) for i in range(parts)]
+    sent += [w_cross(dy) for dy in range(1, ny)]
+    sent += [ho(d, c) for d in range(ny) for c in range(2) if d or c == 0]
     sent += [a1(d) for d in range(ny)] + [a2(d, s) for d in range(1, ny) for s in range(2)]
     for copy in sent:
         copy.wait_send()
@@ -613,6 +679,8 @@
 
     piece = rows // n_tp
     ff = w_gate.shape[2]
+    narrow = width // 2
+    strips = min(8, heads * head // 16)
     dma = pltpu.SemaphoreType.DMA
     vmem = pl.BlockSpec(memory_space=pltpu.VMEM)
     hbm = pl.BlockSpec(memory_space=pl.ANY)
@@ -636,7 +704,7 @@
             pltpu.VMEM((rows, 2 * head), bf16),
             pltpu.VMEM((rows, 2 * head), bf16),
             pltpu.VMEM((tokens, width), bf16),
-            pltpu.VMEM((heads * head, width + SKEW), bf16),
+            pltpu.VMEM((heads * head, narrow + SKEW), bf16),
             pltpu.VMEM((heads * rows, 2 * head), bf16),
             pltpu.VMEM((slots, tokens), bf16),
             pltpu.VMEM((slots, dq), bf16),
@@ -650,20 +718,25 @@
             pltpu.VMEM((heads * rows, 2 * head), jnp.float32),
             pltpu.VMEM((slots, width + SKEW), bf16),
             pltpu.VMEM((slots, ff + SKEW), bf16),
-            pltpu.VMEM((ny, piece, width), bf16),
-            pltpu.VMEM((ny, piece, width), bf16),
-            pltpu.VMEM((ny, piece, width), bf16),
-            pltpu.VMEM((ny, piece, width), bf16),
+            pltpu.VMEM((n_tp * heads * head, width - narrow + SKEW), bf16),
+            pltpu.VMEM((n_tp, piece, heads * head), bf16),
+            pltpu.VMEM((n_tp, piece, heads * head), bf16),
+            pltpu.VMEM((piece, width - narrow), jnp.float32),
+            pltpu.VMEM((ny, piece, narrow), bf16),
+            pltpu.VMEM((ny, piece, narrow), bf16),
+            pltpu.VMEM((ny, piece, narrow), bf16),
+            pltpu.VMEM((ny, piece, narrow), bf16),
             pltpu.VMEM((2, 2, ny, slots // 2, dq), bf16),
             pltpu.VMEM((2, ny, slots // 2, dq), bf16),
             pltpu.VMEM((2, ny, slots // 2, dq), bf16),
             pltpu.VMEM((2, ny, slots // 2, dq), bf16),
             pltpu.VMEM((slots, dq), bf16),
             pltpu.VMEM((slots, dq), bf16),
-            dma((12,)), dma((3,)),
+            dma((13,)), dma((3,)),
             dma((nz + 1,)), dma((nz,)), dma((nz,)), dma((nz,)),
             dma((n_ep,)), dma((n_ep,)), dma((n_ep, ny)), dma((n_ep, ny)),
             dma((2,)), dma((2,)), dma((2, ny)), dma((2, ny)),
+            dma((1,)), dma((1,)), dma((ny, strips)), dma((ny, strips)), dma((ny,)), dma((ny,)), dma((n_tp,)), dma((n_tp,)),
             dma((ny,)), dma((ny,)), dma((ny, 2)), dma((ny, 2)),
             dma((2,)), dma((2,)), dma((2, 2, ny)), dma((2, 2, ny)),
             dma((n_ep,)), dma((n_ep,)),

time: 53.8 us -> 50.4 us (0.937)
  Pallas kernels: 51.3 us -> 47.8 us
    pallas_call x1, Pallas kernels: 51.3 us -> 47.8 us  [per_device(): pl.pallas_call(functools.partial(kernel, (n_ep, n_tp, heads, cap, repeat)...]
where the time goes in v4:
time: 50.4 us; the launch traced here: 49.9 us
  Pallas kernels  47.8 us (95%)
  local copies, waits for them, and re-layouts  1.45 us (3%)
  between operations  0.64 us (1%)
    pallas_call x1, Pallas kernels, per_device(): pl.pallas_call(functools.partial(kernel, (n_ep, n_tp, heads, cap, repeat)...  47.8 us
    unnamed x2, local copies, waits for them, and re-layouts  1.45 us

profile of v4, /device:TPU:0, one launch (start us, length us, event | category | flops | bytes accessed | tf_op | source)
XLA Modules:
  0.0 49.9 jit_solution(1672905596657233974)
XLA Ops:
  0.6 47.8 %shard_map.158 = (bf16[128,2048]{1,0:T(8,128)(2,1)S(1)}, bf16[128,512]{1,0:T(8,128)(2,1)S(1)}) custom-call(s32[2,128]{1,0:T(2,128)} %bitcast.14, f32[2,128]{1,0:T(2,128)} %bitcast.15, f32[1,2048]{1,0:T(1,128)} %bitcast.12, f32[1,2048]{1,0:T(1,128)} %bitcast.13, f32[1,64]{1,0:T(1,128)} %bitcast.16, f32[1,64]{1,0:T(1,128)} %bitcast.17, ...), custom_call_target="tpu_custom_call" | custom-call | tf_op jit(solution)/shard_map/pallas_call | solution.py:687
  48.5 0.8 %copy.19 = bf16[128,2048]{1,0:T(8,128)(2,1)} copy(bf16[128,2048]{1,0:T(8,128)(2,1)S(1)} %get-tuple-element.2) | data formatting | bytes 1048576
  49.3 0.7 %copy.20 = bf16[128,512]{1,0:T(8,128)(2,1)} copy(bf16[128,512]{1,0:T(8,128)(2,1)S(1)} %get-tuple-element.3) | data formatting | bytes 262144

commit v5 on v4

--- a/solution.py
+++ b/solution.py
@@ -42,7 +42,7 @@
     route_ref, logit_ref, pre_ref, gain_ref, qg_ref, kg_ref, turn_ref,
     q_in, k_in, v_in, x_ref, wout_ref, q_ref, placed_ref,
     outgo_ref, mixw_ref, wg, wu, wd, kvbuf, vx, kt, acc, arrived, hidden,
-    wall, ho_out, ho_in, whole, pa, pa_in, pa_red, pa_in2, pm, pm_in, pm_red, pm_in2, summed, ret,
+    mix_high, mix_low, wall, ho_out, ho_in, whole, pa, pa_in, pa_red, pa_in2, pm, pm_in, pm_red, pm_in2, summed, ret,
     in_sem, w_sem, kz_s, kz_r, kx_s, kx_r, disp_s, disp_r, rel_s, rel_r, c0_s, c0_r, cy_s, cy_r,
     w0_s, w0_r, wy_s, wy_r, wc_s, wc_r, ho_s, ho_r, a1_s, a1_r, a2_s, a2_r, m1_s, m1_r, m2_s, m2_r, ret_s, ret_r,
 ):
@@ -98,7 +98,7 @@
     narrow = pa.shape[2]
     wide = wout_hbm.shape[1] - narrow
     dims_here = wout_hbm.shape[0]
-    parts = wy_s.shape[1]
+    parts = min(8, dims_here // 16)
     strip = dims_here // parts
     starts = (parts * 5 // 8, parts * 7 // 8)
 
@@ -112,11 +112,15 @@
 
     def w_row(dy, i):
         block = wall_rows(tp, i, 1)
-        return remote(block, block, wy_s.at[dy, i], wy_r.at[dy, i], ep, same_core(dy))
+        return remote(block, block, wy_s.at[dy - 1], wy_r.at[dy - 1], ep, same_core(dy))
+
+    def w_row_all(dy):
+        block = wall_rows(tp, 0, parts)
+        return remote(block, block, wy_s.at[dy - 1], wy_r.at[dy - 1], ep, same_core(dy))
 
     def w_cross(dy):
         block = wall_rows(row_from(dy) * 2 + core, 0, parts)
-        return remote(block, block, wc_s.at[dy], wc_r.at[dy], ep, partner)
+        return remote(block, block, wc_s.at[dy - 1], wc_r.at[dy - 1], ep, partner)
 
     def w_send(i):
         for dy in range(1, ny):
@@ -241,7 +245,7 @@
 
     disp = {
         d: remote(outgo_ref.at[slot_rows(flip(d))], arrived.at[held(d), lanes_of(tp)],
-                  disp_s.at[d], disp_r.at[d], flip(d), tp)
+                  disp_s.at[0], disp_r.at[d - 1], flip(d), tp)
         for d in range(1, n_ep)
     }
 
@@ -382,7 +386,12 @@
 
     def relay(d, dy):
         block = arrived.at[held(d), lanes_of(tp)]
-        return remote(block, block, rel_s.at[d, dy], rel_r.at[d, dy], ep, same_core(dy))
+        c = 0 if d in groups[0] else 1
+        return remote(block, block, rel_s.at[c, dy - 1], rel_r.at[c, dy - 1], ep, same_core(dy))
+
+    def relay_all(c, dy):
+        block = arrived.at[foreign(c), lanes_of(row_from(dy) * 2 + core)]
+        return remote(block, block, rel_s.at[c, dy - 1], rel_r.at[c, dy - 1], ep, same_core(dy))
 
     def foreign(c):
         count = len(groups[c]) - (1 if 0 in groups[c] else 0)
@@ -392,7 +401,7 @@
         block = arrived.at[foreign(c), lanes_of(row_from(dy) * 2 + core)]
         if dy == 0:
             return remote(block, block, c0_s.at[c], c0_r.at[c], ep, partner)
-        return remote(block, block, cy_s.at[c, dy], cy_r.at[c, dy], ep, partner)
+        return remote(block, block, cy_s.at[c, dy - 1], cy_r.at[c, dy - 1], ep, partner)
 
     def relay_chunk(c):
         for d in groups[c]:
@@ -404,9 +413,7 @@
 
     def cross_chunk(c):
         for dy in range(1, ny):
-            for d in groups[c]:
-                if d:
-                    wait("relay", relay(d, dy))
+            wait("relay", relay_all(c, dy))
             cross(c, dy).start()
 
     ff = wg_hbm.shape[1]
@@ -418,10 +425,13 @@
     def m2(c, s, dy):
         at = pl.ds(s * part, part)
         return remote(pm_red.at[c, lax.rem(row + dy, ny), at], pm_in2.at[c, row, at],
-                      m2_s.at[c, s, dy], m2_r.at[c, s, dy], ep, same_core(dy))
+                      m2_s.at[c, dy - 1], m2_r.at[c, s, dy - 1], ep, same_core(dy))
 
     def chunk_rows(c):
         return slice(c * chunk, (c + 1) * chunk)
+
+    def m2_all(c, dy):
+        return remote(pm_red.at[c, row], pm_in2.at[c, row], m2_s.at[c, dy - 1], m2_r.at[c, 0, dy - 1], ep, partner)
 
     def experts_up(c):
         for dy in range(ny):
@@ -466,7 +476,15 @@
                 m2(c, s, dy).start()
 
     def back(d):
-        return remote(summed.at[held(d)], ret.at[slot_rows(ep)], ret_s.at[d], ret_r.at[d], flip(d), tp)
+        return remote(summed.at[held(d)], ret.at[slot_rows(ep)], ret_s.at[0], ret_r.at[0], flip(d), tp)
+
+    def back_all():
+        at = pl.ds(0, (n_ep - 1) * cap)
+        return remote(summed.at[at], ret.at[at], ret_s.at[0], ret_r.at[0], mate, tp)
+
+    def disp_all():
+        at = pl.ds(0, (n_ep - 1) * cap)
+        return remote(outgo_ref.at[at], summed.at[at], disp_s.at[0], disp_r.at[0], mate, tp)
 
     def send_back(c):
         for s in range(2):
@@ -509,11 +527,18 @@
 
     def a2(d, s):
         at = pl.ds(s * (piece // 2), piece // 2)
-        return remote(pa_red.at[d, at], pa_in2.at[d, at], a2_s.at[d, s], a2_r.at[d, s], ep, same_core(d))
+        return remote(pa_red.at[d, at], pa_in2.at[d, at], a2_s.at[d - 1], a2_r.at[d - 1, s], ep, same_core(d))
+
+    def a2_all(d):
+        return remote(pa_red.at[d], pa_in2.at[d], a2_s.at[d - 1], a2_r.at[d - 1, 0], ep, same_core(d))
 
     def ho(d, c):
         target = lax.rem(row + d, ny) * 2 + (core if c else 1 - core)
-        return remote(ho_out.at[2 * d + c], ho_in.at[tp], ho_s.at[2 * d + c], ho_r.at[2 * d + c], ep, target)
+        return remote(ho_out.at[2 * d + c], ho_in.at[tp], ho_s.at[0], ho_r.at[0], ep, target)
+
+    def ho_all():
+        block = ho_out.at[pl.ds(0, n_tp - 1)]
+        return remote(block, ho_in.at[pl.ds(0, n_tp - 1)], ho_s.at[0], ho_r.at[0], ep, partner)
 
     def finish_start(d):
         sides = finish(lax.rem(row + d, ny))
@@ -534,6 +559,10 @@
         return pa_red[d].astype(f32) + pa_in[d].astype(f32)
 
     attend(ep, True)
+    mixw = mixw_ref[...].T
+    high = mixw.astype(bf16)
+    mix_high[...] = high
+    mix_low[...] = (mixw - high.astype(f32)).astype(bf16)
     relay_chunk(0)
     wait("kv_mate", kv_pass(col))
     attend(mate, False)
@@ -570,7 +599,6 @@
     if not brief:
         line_take(nz - 2)
     reduce_cores(1)
-    send_back(0)
     prepare(line_block(nz - 2), 0)
     prepare(pass_block(nz - 2), 1)
     ins[10].wait()
@@ -578,9 +606,9 @@
     for d in range(1, ny):
         with jax.named_scope("finish"):
             finish_start(d)
+    send_back(0)
     for dy in range(1, ny):
-        for i in range(parts):
-            wait("w_row", w_row(dy, i))
+        wait("w_row", w_row_all(dy))
         w_cross(dy).start()
     for d in range(1, ny):
         pa_red[d] = finish_end(d).astype(bf16)
@@ -593,10 +621,7 @@
     wait("w_partner", w_partner())
     for dy in range(1, ny):
         wait("w_cross", w_cross(dy))
-    for d in range(ny):
-        for c in range(2):
-            if d or c == 0:
-                wait("ho", ho(d, c))
+    wait("ho", ho_all())
     gathered = jnp.concatenate([ho_in[t] for t in range(n_tp)], axis=1)
     whole[...] = jnp.dot(gathered, wall[:, :wide], preferred_element_type=f32)
     for s in range(2):
@@ -611,26 +636,20 @@
         attn_ref[at, :narrow] = (mixed * scale * gain_ref[:, :narrow]).astype(bf16)
         attn_ref[at, narrow:] = (rest * scale * gain_ref[:, narrow:]).astype(bf16)
 
-    for d in range(1, n_ep):
-        wait("back", back(d))
-    mixw = mixw_ref[...]
-    high = mixw.astype(bf16)
-    low = (mixw - high.astype(f32)).astype(bf16)
-    over = (((0,), (0,)), ((), ()))
+    wait("back", back_all())
     moe_ref[...] = (
-        lax.dot_general(high, ret[...], over, preferred_element_type=f32)
-        + lax.dot_general(low, ret[...], over, preferred_element_type=f32)
+        jnp.dot(mix_high[...], ret[...], preferred_element_type=f32)
+        + jnp.dot(mix_low[...], ret[...], preferred_element_type=f32)
     ).astype(bf16)
-    sent = [kv_pass(col)] + list(disp.values())
-    sent += [relay(d, dy) for d in range(1, n_ep) for dy in range(1, ny)]
+
+    sent = [kv_pass(col), disp_all(), back_all(), ho_all(), w_partner()]
+    sent += [relay_all(c, dy) for c in range(2) for dy in range(1, ny)]
     sent += [cross(c, dy) for c in range(2) for dy in range(ny)]
     sent += [m1(c) for c in range(2)]
-    sent += [m2(c, s, dy) for c in range(2) for s in range(2) for dy in range(1, ny)]
-    sent += [back(d) for d in range(1, n_ep)]
-    sent += [w_partner()] + [w_row(dy, i) for dy in range(1, ny) for i in range(parts)]
+    sent += [m2_all(c, dy) for c in range(2) for dy in range(1, ny)]
+    sent += [w_row_all(dy) for dy in range(1, ny)]
     sent += [w_cross(dy) for dy in range(1, ny)]
-    sent += [ho(d, c) for d in range(ny) for c in range(2) if d or c == 0]
-    sent += [a1(d) for d in range(ny)] + [a2(d, s) for d in range(1, ny) for s in range(2)]
+    sent += [a1(d) for d in range(ny)] + [a2_all(d) for d in range(1, ny)]
     for copy in sent:
         copy.wait_send()
 
@@ -653,6 +672,17 @@
         return carry
 
     lax.fori_loop(0, nz - 1, kv_done, 0)
+
+
+def hand_over(attn_ref, moe_ref, attn_hbm, moe_hbm, sem):
+    copies = [
+        pltpu.make_async_copy(attn_ref, attn_hbm, sem.at[0]),
+        pltpu.make_async_copy(moe_ref, moe_hbm, sem.at[1]),
+    ]
+    for copy in copies:
+        copy.start()
+    for copy in copies:
+        copy.wait()
 
 
 def per_device(
@@ -679,12 +709,11 @@
 
     piece = rows // n_tp
     ff = w_gate.shape[2]
-    narrow = width // 2
-    strips = min(8, heads * head // 16)
+    narrow = width * 4 // 8
     dma = pltpu.SemaphoreType.DMA
     vmem = pl.BlockSpec(memory_space=pltpu.VMEM)
     hbm = pl.BlockSpec(memory_space=pl.ANY)
-    return pl.pallas_call(
+    outs = pl.pallas_call(
         functools.partial(kernel, (n_ep, n_tp, heads, cap, repeat)),
         out_shape=(
             pltpu.VMEM((piece, width), bf16),
@@ -718,6 +747,8 @@
             pltpu.VMEM((heads * rows, 2 * head), jnp.float32),
             pltpu.VMEM((slots, width + SKEW), bf16),
             pltpu.VMEM((slots, ff + SKEW), bf16),
+            pltpu.VMEM((tokens, slots), bf16),
+            pltpu.VMEM((tokens, slots), bf16),
             pltpu.VMEM((n_tp * heads * head, width - narrow + SKEW), bf16),
             pltpu.VMEM((n_tp, piece, heads * head), bf16),
             pltpu.VMEM((n_tp, piece, heads * head), bf16),
@@ -734,12 +765,12 @@
             pltpu.VMEM((slots, dq), bf16),
             dma((13,)), dma((3,)),
             dma((nz + 1,)), dma((nz,)), dma((nz,)), dma((nz,)),
-            dma((n_ep,)), dma((n_ep,)), dma((n_ep, ny)), dma((n_ep, ny)),
-            dma((2,)), dma((2,)), dma((2, ny)), dma((2, ny)),
-            dma((1,)), dma((1,)), dma((ny, strips)), dma((ny, strips)), dma((ny,)), dma((ny,)), dma((n_tp,)), dma((n_tp,)),
-            dma((ny,)), dma((ny,)), dma((ny, 2)), dma((ny, 2)),
-            dma((2,)), dma((2,)), dma((2, 2, ny)), dma((2, 2, ny)),
-            dma((n_ep,)), dma((n_ep,)),
+            dma((1,)), dma((n_ep - 1,)), dma((2, ny - 1)), dma((2, ny - 1)),
+            dma((2,)), dma((2,)), dma((2, ny - 1)), dma((2, ny - 1)),
+            dma((1,)), dma((1,)), dma((ny - 1,)), dma((ny - 1,)), dma((ny - 1,)), dma((ny - 1,)), dma((1,)), dma((1,)),
+            dma((ny,)), dma((ny,)), dma((ny - 1,)), dma((ny - 1, 2)),
+            dma((2,)), dma((2,)), dma((2, ny - 1)), dma((2, 2, ny - 1)),
+            dma((1,)), dma((1,)),
         ],
         compiler_params=pltpu.CompilerParams(
             collective_id=0, has_side_effects=True, vmem_limit_bytes=VMEM_LIMIT
@@ -748,6 +779,17 @@
         routes.T, route_logits.T, pre_gain[None, :], post_gain[None, :], q_gain[None, :], k_gain[None, :], turns,
         q_in, k_in, v_in, moe_in, w_out, w_gate[0], w_up[0], w_down[0],
     )
+    return pl.pallas_call(
+        hand_over,
+        out_shape=(
+            jax.ShapeDtypeStruct((piece, width), bf16),
+            jax.ShapeDtypeStruct((tokens, dq), bf16),
+        ),
+        in_specs=[vmem, vmem],
+        out_specs=(hbm, hbm),
+        scratch_shapes=[dma((2,))],
+        compiler_params=pltpu.CompilerParams(vmem_limit_bytes=2 * 1024 * 1024),
+    )(*outs)
 
 
 def solution(mesh):

time: 50.4 us -> 48.9 us (0.970)
  local copies, waits for them, and re-layouts: 1.45 us -> 0 us
    unnamed x2 -> x0, local copies, waits for them, and re-layouts: 1.45 us -> none
    pallas_call x1, Pallas kernels: 47.8 us -> 46.5 us  [per_device(): pl.pallas_call(functools.partial(kernel, (n_ep, n_tp, heads, cap, repeat)...]
    pallas_call x0 -> x1, Pallas kernels: none -> 0.85 us  [per_device(): pl.pallas_call(hand_over, out_shape=(jax.ShapeDtypeStruct((piece, width),...]
where the time goes in v5:
time: 48.9 us; the launch traced here: 48.1 us
  Pallas kernels  47.3 us (97%)
  between operations  0.8 us (2%)
    pallas_call x1, Pallas kernels, per_device(): pl.pallas_call(functools.partial(kernel, (n_ep, n_tp, heads, cap, repeat)...  46.5 us

profile of v5, /device:TPU:0, one launch (start us, length us, event | category | flops | bytes accessed | tf_op | source)
XLA Modules:
  0.0 48.1 jit_solution(13424930784673200514)
XLA Ops:
  0.6 46.5 %shard_map.158 = (bf16[128,2048]{1,0:T(8,128)(2,1)S(1)}, bf16[128,512]{1,0:T(8,128)(2,1)S(1)}) custom-call(s32[2,128]{1,0:T(2,128)} %bitcast.14, f32[2,128]{1,0:T(2,128)} %bitcast.15, f32[1,2048]{1,0:T(1,128)} %bitcast.12, f32[1,2048]{1,0:T(1,128)} %bitcast.13, f32[1,64]{1,0:T(1,128)} %bitcast.16, f32[1,64]{1,0:T(1,128)} %bitcast.17, ...), custom_call_target="tpu_custom_call" | custom-call | tf_op jit(solution)/shard_map/pallas_call | solution.py:716
  47.1 0.8 %shard_map.159 = (bf16[128,2048]{1,0:T(8,128)(2,1)}, bf16[128,512]{1,0:T(8,128)(2,1)}) custom-call(bf16[128,2048]{1,0:T(8,128)(2,1)S(1)} %get-tuple-element.4.attn_ref, bf16[128,512]{1,0:T(8,128)(2,1)S(1)} %get-tuple-element.5.moe_ref), custom_call_target="tpu_custom_call" | custom-call | tf_op jit(solution)/shard_map/pallas_call | solution.py:782

commit v6 on v5

--- a/solution.py
+++ b/solution.py
@@ -100,7 +100,7 @@
     dims_here = wout_hbm.shape[0]
     parts = min(8, dims_here // 16)
     strip = dims_here // parts
-    starts = (parts * 5 // 8, parts * 7 // 8)
+    starts = (parts * 4 // 8, parts * 8 // 8)
 
     def wall_rows(t, i, count):
         first_row = pl.multiple_of(t * dims_here + i * strip, strip)
@@ -155,14 +155,12 @@
             (wout_hbm.at[:, pl.ds(narrow, wide)], wall_rows(tp, 0, parts)),
         ))
     ]
-    for copy in ins:
+    for copy in ins[:8] + ins[12:]:
         copy.start()
     loads = [
         pltpu.make_async_copy(src, dst, w_sem.at[i])
         for i, (src, dst) in enumerate(((wg_hbm, wg.at[:, cols_of(wg_hbm)]), (wu_hbm, wu.at[:, cols_of(wu_hbm)]), (wd_hbm, wd.at[:, cols_of(wd_hbm)])))
     ]
-    for copy in loads:
-        copy.start()
     barrier = pltpu.get_barrier_semaphore()
     for d in range(1, n_ep):
         pl.semaphore_signal(barrier, inc=1, device_id=(ep_at(d), tp), device_id_type=MESH)
@@ -232,6 +230,8 @@
     odd = lax.rem(kv_index, 2)
     for copy in ins[4:8]:
         copy.wait()
+    for copy in ins[8:12] + loads:
+        copy.start()
     k_gain = jnp.concatenate([kg_ref[...], kg_ref[...]], axis=1)
     for b in range(blocks):
         at = slice(b * GRID_W, (b + 1) * GRID_W)
@@ -588,10 +588,10 @@
     reduce_cores(0)
     for i in range(starts[1], parts):
         w_send(i)
+    if brief:
+        line_end(False)
     with jax.named_scope("up1"):
         experts_up(1)
-    if brief:
-        line_end(False)
     with jax.named_scope("down1"):
         experts_down(1)
     attend(pass_block(split), False)

time: 48.9 us -> 48.3 us (0.988); the launches traced: 48.1 us -> 48.1 us
  no operation moved by 1% of the time
where the time goes in v6:
time: 48.3 us; the launch traced here: 48.1 us
  Pallas kernels  47.3 us (98%)
  between operations  0.8 us (2%)
    pallas_call x1, Pallas kernels, per_device(): pl.pallas_call(functools.partial(kernel, (n_ep, n_tp, heads, cap, repeat)...  46.5 us

profile of v6, /device:TPU:0, one launch (start us, length us, event | category | flops | bytes accessed | tf_op | source)
XLA Modules:
  0.0 48.1 jit_solution(653915149828427366)
XLA Ops:
  0.6 46.5 %shard_map.158 = (bf16[128,2048]{1,0:T(8,128)(2,1)S(1)}, bf16[128,512]{1,0:T(8,128)(2,1)S(1)}) custom-call(s32[2,128]{1,0:T(2,128)} %bitcast.14, f32[2,128]{1,0:T(2,128)} %bitcast.15, f32[1,2048]{1,0:T(1,128)} %bitcast.12, f32[1,2048]{1,0:T(1,128)} %bitcast.13, f32[1,64]{1,0:T(1,128)} %bitcast.16, f32[1,64]{1,0:T(1,128)} %bitcast.17, ...), custom_call_target="tpu_custom_call" | custom-call | tf_op jit(solution)/shard_map/pallas_call | solution.py:716
  47.1 0.8 %shard_map.159 = (bf16[128,2048]{1,0:T(8,128)(2,1)}, bf16[128,512]{1,0:T(8,128)(2,1)}) custom-call(bf16[128,2048]{1,0:T(8,128)(2,1)S(1)} %get-tuple-element.4.attn_ref, bf16[128,512]{1,0:T(8,128)(2,1)S(1)} %get-tuple-element.5.moe_ref), custom_call_target="tpu_custom_call" | custom-call | tf_op jit(solution)/shard_map/pallas_call | solution.py:782
